TPU v7x, 256 devices: a whole 4x4x8 slice. The times are simulated.
256 devices in a mesh: ep: 32 (over z, x), tp: 8 (over y, core).
Axes of the slice: x: 4, y: 4, z: 8, core: 2. Of those that a mesh axis runs over, the one named last changes fastest.
Arguments:
- tokens: bfloat16 [2048, 2048], P('ep'), may hold values from -6 to 6
- norm_gain: float32 [2048], replicated, may hold values from 0.1 to 1.9
- norm_shift: float32 [2048], replicated, may hold values from -3 to 3
- expert_ids: int32 [2048, 4], P('ep'), may hold values from 0 to 63, as said below
- gate_weights: float32 [2048, 4], P('ep'), may hold values from 0.1 to 1
- expert_gate: bfloat16 [64, 2048, 512], P('ep', None, 'tp'), may hold values from -0.125 to 0.125
- expert_up: bfloat16 [64, 2048, 512], P('ep', None, 'tp'), may hold values from -0.125 to 0.125
- expert_down: bfloat16 [64, 512, 2048], P('ep', 'tp'), may hold values from -0.25 to 0.25
Outputs:
- mixed_out: bfloat16 [2048, 2048], P('ep', 'tp')
Inputs may be any that keep to these rules, and one draw needn't show every extreme that they name: `expert_ids`: each row names 4 distinct experts that all lie in one group of 16 consecutive expert numbers. In the rows of one index of ep (aligned blocks of 64 rows) no expert is named by more than 8 rows, and in every block some expert is named by exactly 8 rows.
All inputs are finite; a program needn't handle non-finite values.
Results may differ from a plain program's by a relative error of at most 0.002.
Values may be sent and summed in bfloat16 or wider, within the bound.
A program may use at most 64 MiB of HBM per device.

v0:
```python
import jax
import jax.numpy as jnp
from jax import lax
from jax.sharding import PartitionSpec as P

GROUPS = 4


epsilon = 1e-05


def folded(array, axis, dim, absorb, carry):
    whole = jax.tree.map(lambda part: lax.all_gather(part, axis, axis=dim, tiled=True), array)
    return absorb(carry, whole, jnp.int32(0))


def layer_norm(tokens, norm_gain, norm_shift):
    values = tokens.astype(jnp.float32)
    centre = jnp.mean(values, axis=-1, keepdims=True)
    spread = jnp.mean(jnp.square(values - centre), axis=-1, keepdims=True)
    scaled = (values - centre) * lax.rsqrt(spread + epsilon) * norm_gain + norm_shift
    return scaled.astype(jnp.bfloat16)


def per_device(
    tokens, norm_gain, norm_shift, expert_ids, gate_weights, expert_gate, expert_up, expert_down
):
    tok_rows, features = tokens.shape
    top_count = expert_ids.shape[1]
    local_count = expert_gate.shape[0]
    ep_size = lax.axis_size("ep")
    tp_size = lax.axis_size("tp")
    total_experts = local_count * ep_size
    group_size = total_experts // GROUPS
    capacity = tok_rows // 2 * top_count // group_size
    recv_rows = ep_size * capacity
    normed = layer_norm(tokens, norm_gain, norm_shift)
    flat_ids = expert_ids.reshape(-1)
    onehot = (flat_ids[:, None] == jnp.arange(total_experts, dtype=jnp.int32)[None, :]).astype(
        jnp.int32
    )
    before = jnp.cumsum(onehot, axis=0) - onehot
    slot_index = jnp.sum(before * onehot, axis=1)
    positions = flat_ids * capacity + slot_index
    source_rows = jnp.repeat(normed, top_count, axis=0)
    packed = (
        jnp.zeros((total_experts * capacity, features), jnp.bfloat16).at[positions].set(source_rows)
    )

    def to_experts(received):
        columns = received.shape[-1]
        arranged = received.reshape(ep_size, local_count, capacity, columns).transpose(1, 0, 2, 3)
        return arranged.reshape(local_count, recv_rows, columns)

    def to_sources(result):
        columns = result.shape[-1]
        arranged = result.reshape(local_count, ep_size, capacity, columns).transpose(1, 0, 2, 3)
        return arranged.reshape(total_experts * capacity, columns)

    feature_share = features // tp_size
    own_part = lax.dynamic_slice_in_dim(
        packed, lax.axis_index("tp") * feature_share, feature_share, 1
    )
    arrived = to_experts(lax.all_to_all(own_part, "ep", split_axis=0, concat_axis=0, tiled=True))
    zero_init = jnp.zeros((local_count, recv_rows, expert_gate.shape[2]), jnp.float32)

    def add_both(totals, portion, offset):
        piece_rows = portion.shape[2]
        rows_gate = lax.dynamic_slice_in_dim(expert_gate, offset, piece_rows, 1)
        rows_up = lax.dynamic_slice_in_dim(expert_up, offset, piece_rows, 1)
        first = totals[0] + jnp.einsum(
            "erd,edf->erf", portion, rows_gate, preferred_element_type=jnp.float32
        )
        second = totals[1] + jnp.einsum(
            "erd,edf->erf", portion, rows_up, preferred_element_type=jnp.float32
        )
        return (first, second)

    gate_sum, upward = folded(arrived, "tp", 2, add_both, (zero_init, zero_init))
    hidden = (jax.nn.silu(gate_sum) * upward).astype(jnp.bfloat16)
    partial_out = jnp.einsum(
        "erf,efd->erd", hidden, expert_down, preferred_element_type=jnp.float32
    )
    weights_flat = gate_weights.reshape(-1)

    def combine(returned):
        picked = returned[positions] * weights_flat[:, None]
        return jnp.sum(picked.reshape(tok_rows, top_count, picked.shape[-1]), axis=1)

    reduced = lax.psum_scatter(partial_out, "tp", scatter_dimension=2, tiled=True)
    returned = lax.all_to_all(to_sources(reduced), "ep", split_axis=0, concat_axis=0, tiled=True)
    mixed_out = combine(returned)
    return mixed_out.astype(jnp.bfloat16)


def solution(mesh):
    return jax.shard_map(
        per_device,
        mesh=mesh,
        in_specs=(
            P("ep", None),
            P(),
            P(),
            P("ep", None),
            P("ep", None),
            P("ep", None, "tp"),
            P("ep", None, "tp"),
            P("ep", "tp", None),
        ),
        out_specs=P("ep", "tp"),
        check_vma=False,
    )
```

profile of v0, /device:TPU:25, one launch (start us, length us, event | category | flops | bytes accessed | tf_op | source)
XLA Modules:
  0.0 150.8 jit_solution(10570310799276013756)
XLA Ops:
  6.5 0.8 copy.11
  7.4 0.1 eq.29
  7.5 0.1 eq.25
  7.6 0.7 broadcast_multiply_fusion
  8.3 0.6 reduce-window.6
  8.9 0.2 slice_reduce_fusion
  9.2 0.1 mul.56
  9.3 1.1 convert_reduce_fusion
  10.4 1.2 fusion.6
  11.6 1.1 fusion.9
  12.8 0.5 broadcast_in_dim.5
  13.3 1.1 reshape.104
  14.5 3.5 %scatter_custom_fusion = bf16[512,2048]{1,0:T(8,128)(2,1)S(1)} fusion(s32[256]{0:T(256)S(1)} %bitcast.45, bf16[256,2048]{1,0:T(8,128)(2,1)} %reshape.104, bf16[]{:T(256)} %constant.11.clone.1), kind=kCustom, calls=%fused_computation.5 | custom fusion | bytes 2097664 | tf_op jit(solution)/shard_map/scatter | solution.py:47
  18.1 22.7 %all_to_all.21 = bf16[32,16,256]{2,1,0:T(8,128)(2,1)S(1)} all-to-all(bf16[32,16,256]{2,1,0:T(8,128)(2,1)S(1)} %bitcast.43), channel_id=1, replica_groups=mesh['ep'=32,'tp'=8] {'ep'}, dimensions={0} | all-to-all | bytes 524288 | tf_op jit(solution)/shard_map/all_to_all | solution.py:64
  40.8 0.7 copy_bitcast_fusion.1
  41.6 25.4 %all-gather.2.cloned.1.call-done = bf16[2,256,2048]{2,1,0:T(8,128)(2,1)} async-done(((bf16[2,256,256]{2,1,0:T(8,128)(2,1)}), bf16[2,256,2048]{2,1,0:T(8,128)(2,1)}) %all-gather.2.cloned.1.call-update) | async-done | bytes 2097168 | tf_op jit(solution)/shard_map/all_gather | solution.py:13
  67.0 2.6 %fusion.21 = f32[2,256,64]{1,2,0:T(8,128)S(1)} fusion(bf16[2,256,2048]{2,1,0:T(8,128)(2,1)} %all-gather.2.cloned.1.call-done, bf16[2,2048,64]{1,2,0:T(8,128)(2,1)} %param.13), kind=kOutput, calls=%fused_computation.40 | convolution fusion | flops 134217728 | bytes 2752512 | tf_op jit(solution)/shard_map/erd,edf->erf/dot_general | solution.py:71
  69.6 3.4 %fusion.1 = f32[2,256,2048]{2,1,0:T(8,128)} fusion(bf16[2,64,2048]{2,1,0:T(8,128)(2,1)S(1)} %copy-done, bf16[2,256,2048]{2,1,0:T(8,128)(2,1)S(1)} %copy-done.1, bf16[2,2048,64]{1,2,0:T(8,128)(2,1)S(1)} %copy-done.2, f32[2,256,64]{1,2,0:T(8,128)S(1)} %fusion.21), kind=kOutput, calls=%fused_computation.4 | convolution fusion | flops 268632064 | bytes 7471104 | tf_op jit(solution)/shard_map/erf,efd->erd/dot_general | solution.py:81
  73.1 40.5 %reduce-scatter.2.cloned.1.call-done = f32[2,256,256]{2,1,0:T(8,128)} async-done(((f32[2,256,2048]{2,1,0:T(8,128)}), f32[2,256,256]{2,1,0:T(8,128)}) %reduce-scatter.2.cloned.1.call-update) | async-done | bytes 524304 | tf_op jit(solution)/shard_map/reduce_scatter | solution.py:90
  113.5 1.9 %copy_bitcast_fusion = f32[32,16,256]{2,1,0:T(8,128)} fusion(f32[2,256,256]{2,1,0:T(8,128)} %reduce-scatter.2.cloned.1.call-done), kind=kLoop, calls=%fused_computation.15 | loop fusion | bytes 1048576 | tf_op jit(solution)/shard_map/all_to_all | solution.py:91
  115.4 9.3 %all-to-all-start.1 = ((f32[32,16,256]{2,1,0:T(8,128)}), f32[32,16,256]{2,1,0:T(8,128)S(1)}, u32[]{:S(2)}, u32[]{:S(2)}) async-start(f32[32,16,256]{2,1,0:T(8,128)} %copy_bitcast_fusion), calls=%async_computation.2 | async-start | bytes 1048576 | tf_op jit(solution)/shard_map/all_to_all | solution.py:91
  124.9 17.2 %all-to-all-done.1 = f32[32,16,256]{2,1,0:T(8,128)S(1)} async-done(((f32[32,16,256]{2,1,0:T(8,128)}), f32[32,16,256]{2,1,0:T(8,128)S(1)}, u32[]{:S(2)}, u32[]{:S(2)}) %all-to-all-start.1) | async-done | bytes 524320 | tf_op jit(solution)/shard_map/all_to_all | solution.py:91
  142.1 1.0 gather_fusion
  143.1 0.9 multiply_reduce_fusion
  (24 shorter events, 0.6 us)
Async XLA Ops:
  6.5 63.0 %copy-start = (bf16[2,64,2048]{2,1,0:T(8,128)(2,1)S(1)}, bf16[2,64,2048]{2,1,0:T(8,128)(2,1)}, u32[]{:S(2)}) copy-start(bf16[2,64,2048]{2,1,0:T(8,128)(2,1)} %param.15) | copy-start | bytes 1572868
  6.5 60.5 %all-gather.2.cloned.1.call-start = ((), (), s32[]{:S(2)}) async-start(), calls=%async_computation.3 | async-start | bytes 2359296 | tf_op jit(solution)/shard_map/all_gather | solution.py:13
  18.1 51.5 %copy-start.2 = (bf16[2,2048,64]{1,2,0:T(8,128)(2,1)S(1)}, bf16[2,2048,64]{1,2,0:T(8,128)(2,1)}, u32[]{:S(2)}) copy-start(bf16[2,2048,64]{1,2,0:T(8,128)(2,1)} %param.14) | copy-start | bytes 1572868
  41.5 72.0 %reduce-scatter.2.cloned.1.call-start = ((), (), s32[]{:S(2)}) async-start(), calls=%async_computation.4 | async-start | bytes 4718592 | tf_op jit(solution)/shard_map/reduce_scatter | solution.py:90
  67.0 2.6 %copy-start.1 = (bf16[2,256,2048]{2,1,0:T(8,128)(2,1)S(1)}, bf16[2,256,2048]{2,1,0:T(8,128)(2,1)}, u32[]{:S(2)}) copy-start(bf16[2,256,2048]{2,1,0:T(8,128)(2,1)} %all-gather.2.cloned.1.call-done) | copy-start | bytes 6291460
  73.0 51.7 %copy-start.3 = (f32[64,4]{0,1:T(4,128)S(1)}, f32[64,4]{0,1:T(4,128)}, u32[]{:S(2)}) copy-start(f32[64,4]{0,1:T(4,128)} %param.12) | copy-start | bytes 3076
  115.4 26.6 %all-to-all-start.1 = ((f32[32,16,256]{2,1,0:T(8,128)}), f32[32,16,256]{2,1,0:T(8,128)S(1)}, u32[]{:S(2)}, u32[]{:S(2)}) async-start(f32[32,16,256]{2,1,0:T(8,128)} %copy_bitcast_fusion), calls=%async_computation.2 | async-start | bytes 1048576 | tf_op jit(solution)/shard_map/all_to_all | solution.py:91
Sparse Core Ops, SparseCore 0:
  41.7 25.2 all-gather.1
  73.2 40.3 reduce-scatter.1
where the time goes:
time: 151 us
  waiting for transfers between devices  83.1 us (55%)
  blocking collectives  22.7 us (15%)
  between operations  13.5 us (9%)
  local copies, waits for them, and re-layouts  10.4 us (7%)
  starting transfers between devices  9.38 us (6%)
  matrix products  5.99 us (4%)
  other arithmetic  5.74 us (4%)
    reduce_scatter x1, waiting for transfers between devices, per_device(): lax.psum_scatter(partial_out, 'tp', scatter_dimension=2, tiled=True)  40.5 us
    all_gather x1, waiting for transfers between devices, folded(): lax.all_gather(part, axis, axis=dim, tiled=True)  25.4 us
    all_to_all x1, blocking collectives, per_device(): lax.all_to_all(own_part, 'ep', split_axis=0, concat_axis=0, tiled=True)  22.7 us
    all_to_all x1, waiting for transfers between devices, per_device(): lax.all_to_all(to_sources(reduced), 'ep', split_axis=0, concat_axis=0, ti...  17.2 us
    all_to_all x1, starting transfers between devices, per_device(): lax.all_to_all(to_sources(reduced), 'ep', split_axis=0, concat_axis=0, ti...  9.34 us
    scatter x1, local copies, waits for them, and re-layouts, per_device(): jnp.zeros((total_experts * capacity, features), jnp.bfloat16).at[positions]  3.5 us
    dot_general x1, matrix products, per_device(): jnp.einsum('erf,efd->erd', hidden, expert_down, preferred_element_type=jn...  3.42 us
  transfers between devices with their start and end apart: 3, of which 3 were waited for; matrix products, arithmetic and copies ran while one was open for 0% of the time, Pallas kernels for 0%

commit v1 on v0

v1 whole, which is shorter than its diff:
```python
import functools

import jax
import jax.numpy as jnp
from jax import lax
from jax.experimental import pallas as pl
from jax.experimental.pallas import tpu as pltpu
from jax.sharding import PartitionSpec as P

MESH = pl.DeviceIdType.MESH
GROUPS = 4
NZ, NX, NY, NC = 8, 4, 4, 2
NE, NT = NZ * NX, NY * NC
CHUNKS = 4
PER = NE // CHUNKS
epsilon = 1e-05
F32, BF16 = jnp.float32, jnp.bfloat16


def offsets(n):
    q, r = n // PER, n % PER
    half, dx = r // NX, r % NX
    return q + half * (NZ - 1 - 2 * q), dx


def kernel(
    tokens_h, gain_v, shift_v, ids_v, gw_v, gate_h, up_h, down_h, out_v,
    tok, wall, packed, gath, wd, hid, outb, ret, combine,
    load_sem, disp_send, disp_recv, ag_send, ag_recv, wd_send, wd_recv, hid_send, hid_recv, ret_send, ret_recv,
):
    ep, tp = lax.axis_index("ep"), lax.axis_index("tp")
    ez, ex = ep // NX, ep % NX
    ty, tc = tp // NC, tp % NC
    mate = ty * NC + 1 - tc
    rows, features = tok.shape
    share = features // NT
    block = packed.shape[0] // NE
    half = wall.shape[1]

    def source_of(n):
        dz, dx = offsets(n)
        return ((ez + dz) % NZ) * NX + (ex + dx) % NX

    def dest_of(n):
        dz, dx = offsets(n)
        return ((ez + NZ - dz) % NZ) * NX + (ex + NX - dx) % NX

    barrier = pltpu.get_barrier_semaphore()

    @pl.loop(1, NE)
    def _(d):
        pl.semaphore_signal(barrier, inc=1, device_id=((ep + d) % NE, tp), device_id_type=MESH)

    @pl.loop(1, NT)
    def _(d):
        pl.semaphore_signal(barrier, inc=1, device_id=(ep, (tp + d) % NT), device_id_type=MESH)

    def tp_cols(t):
        return pl.ds(pl.multiple_of(t * share, share), share)

    load_tok = pltpu.make_async_copy(tokens_h, tok, load_sem.at[0])
    load_gate = pltpu.make_async_copy(gate_h, wall.at[pl.ds(0, 2)], load_sem.at[1])
    load_up = pltpu.make_async_copy(up_h, wall.at[pl.ds(2, 2)], load_sem.at[2])
    load_down = pltpu.make_async_copy(down_h.at[:, :, tp_cols(tp)], wd.at[tp], load_sem.at[3])
    load_tok.start()
    load_gate.start()
    load_up.start()
    load_down.start()

    experts = NE * (wall.shape[0] // 2)
    cap = NE * block // experts
    ids, gw = ids_v[...], gw_v[...]
    numbers = lax.broadcasted_iota(jnp.int32, (experts, rows), 0)
    hits = jnp.zeros((experts, rows), F32)
    weights = jnp.zeros((experts, rows), F32)
    for k in range(ids.shape[0]):
        same = ids[k : k + 1, :] == numbers
        hits = hits + jnp.where(same, 1.0, 0.0)
        weights = weights + jnp.where(same, gw[k : k + 1, :], 0.0)
    earlier = lax.broadcasted_iota(jnp.int32, (rows, rows), 0) < lax.broadcasted_iota(jnp.int32, (rows, rows), 1)
    before = jnp.dot(hits.astype(BF16), jnp.where(earlier, 1.0, 0.0).astype(BF16), preferred_element_type=F32)
    code = (hits * (before + 1.0)).astype(BF16)
    slots = experts * cap
    spread = (
        lax.broadcasted_iota(jnp.int32, (slots, experts), 0) // cap
        == lax.broadcasted_iota(jnp.int32, (slots, experts), 1)
    )
    spread_f = jnp.where(spread, 1.0, 0.0)
    wanted = (lax.broadcasted_iota(jnp.int32, (slots, rows), 0) % cap + 1).astype(F32)
    place = jnp.dot(spread_f.astype(BF16), code, preferred_element_type=F32) == wanted
    w_slots = jnp.dot(spread_f, weights, preferred_element_type=F32, precision=lax.Precision.HIGHEST)
    combine[...] = jnp.where(place, w_slots, 0.0).T

    load_tok.wait()
    values = tok[...].astype(F32)
    centre = jnp.mean(values, axis=-1, keepdims=True)
    spread_t = jnp.mean(jnp.square(values - centre), axis=-1, keepdims=True)
    own = tok[:, tp_cols(tp)].astype(F32)
    normed = (own - centre) * lax.rsqrt(spread_t + epsilon) * gain_v[:, tp_cols(tp)] + shift_v[:, tp_cols(tp)]
    normed = normed.astype(BF16)
    packed[...] = jnp.dot(jnp.where(place, 1.0, 0.0).astype(BF16), normed, preferred_element_type=F32).astype(BF16)
    gath[tp, 0, :block, :] = packed[pl.ds(pl.multiple_of(ep * block, block), block), :]

    pl.semaphore_wait(barrier, NE - 1 + NT - 1)

    @pl.loop(1, NE)
    def _(n):
        dest = dest_of(n)
        pltpu.make_async_remote_copy(
            src_ref=packed.at[pl.ds(pl.multiple_of(dest * block, block), block)],
            dst_ref=gath.at[tp, n // PER, pl.ds(pl.multiple_of((n % PER) * block, block), block)],
            send_sem=disp_send,
            recv_sem=disp_recv.at[n // PER],
            device_id=(dest, tp),
            device_id_type=MESH,
        ).start()

    @pl.loop(1, NT)
    def _(d):
        t = (tp + d) % NT
        pltpu.make_async_remote_copy(
            src_ref=down_h.at[:, :, tp_cols(t)],
            dst_ref=wd.at[tp],
            send_sem=wd_send,
            recv_sem=wd_recv,
            device_id=(ep, t),
            device_id_type=MESH,
        ).start()

    def arrived(ref, sem):
        pltpu.make_async_copy(ref, ref, sem).wait()

    def share_out(buf, slot, q, send, recv, t):
        pltpu.make_async_remote_copy(
            src_ref=buf.at[slot, q],
            dst_ref=buf.at[slot, q],
            send_sem=send,
            recv_sem=recv.at[slot, q],
            device_id=(ep, t),
            device_id_type=MESH,
        ).start()

    def spread_own(buf, q, send, recv):
        for dy in (2, 1, 3):
            share_out(buf, tp, q, send, recv, ((ty + dy) % NY) * NC + tc)
        share_out(buf, tp, q, send, recv, mate)

    def forward(buf, q, send, recv):
        for dy in (1, 3, 2):
            slot = ((ty + dy) % NY) * NC + tc
            arrived(buf.at[slot, q], recv.at[slot, q])
            share_out(buf, slot, q, send, recv, mate)

    def from_mate(buf, q, recv):
        for dy in (0, 1, 3, 2):
            slot = ((ty + dy) % NY) * NC + 1 - tc
            arrived(buf.at[slot, q], recv.at[slot, q])

    chunk_rows = PER * block

    def stage_a(q):
        if q == 0:
            part = gath.at[tp, 0, pl.ds(block, chunk_rows - block)]
        else:
            part = gath.at[tp, q]
        arrived(part, disp_recv.at[q])
        spread_own(gath, q, ag_send, ag_recv)

    def stage_b(q):
        forward(gath, q, ag_send, ag_recv)

    def stage_c(q):
        if q == 0:
            load_gate.wait()
            load_up.wait()
        from_mate(gath, q, ag_recv)
        x = jnp.concatenate([gath[s, q] for s in range(NT)], axis=-1)
        both = lax.dot_general(
            x, wall[...].reshape(4 * half, features), (((1,), (1,)), ((), ())), preferred_element_type=F32
        )
        g, u = both[:, : 2 * half], both[:, 2 * half :]
        h = g / (1.0 + jnp.exp(-g)) * u
        row = lax.broadcasted_iota(jnp.int32, h.shape, 0)
        lane = lax.broadcasted_iota(jnp.int32, h.shape, 1)
        hid[tp, q] = jnp.where((row % block) // cap == lane // half, h, 0.0).astype(BF16)
        spread_own(hid, q, hid_send, hid_recv)

    def stage_d(q):
        forward(hid, q, hid_send, hid_recv)

    def stage_e(q):
        if q == 0:
            load_down.wait()
            arrived(wd.at[pl.ds(0, NT - 1)], wd_recv)
        from_mate(hid, q, hid_recv)
        x = jnp.concatenate([hid[s, q] for s in range(NT)], axis=-1)
        result = jnp.dot(x, wd[...].reshape(NT * 2 * half, share), preferred_element_type=F32)
        outb[q] = result
        if q == 0:
            ret[ep] = result[:block]

        @pl.loop(1 if q == 0 else 0, PER)
        def _(r):
            dest = source_of(q * PER + r)
            pltpu.make_async_remote_copy(
                src_ref=outb.at[q, pl.ds(pl.multiple_of(r * block, block), block)],
                dst_ref=ret.at[ep],
                send_sem=ret_send,
                recv_sem=ret_recv,
                device_id=(dest, tp),
                device_id_type=MESH,
            ).start()

    stages = (stage_a, stage_b, stage_c, stage_d, stage_e)
    for step in range(CHUNKS + len(stages) - 1):
        for lag, stage in enumerate(stages):
            if 0 <= step - lag < CHUNKS:
                stage(step - lag)

    arrived(ret.at[pl.ds(0, NE - 1)], ret_recv)
    back = ret[...].reshape(NE * block, share)
    out_v[...] = jnp.dot(
        combine[...], back, preferred_element_type=F32, precision=lax.Precision.HIGHEST
    ).astype(BF16)

    arrived(packed.at[pl.ds(0, (NE - 1) * block)], disp_send)
    arrived(wd.at[pl.ds(0, NT - 1)], wd_send)
    arrived(gath.at[pl.ds(0, NT - 1)], ag_send)
    arrived(hid.at[pl.ds(0, NT - 1)], hid_send)
    arrived(ret.at[pl.ds(0, NE - 1)], ret_send)


def per_device(tokens, norm_gain, norm_shift, expert_ids, gate_weights, expert_gate, expert_up, expert_down):
    rows, features = tokens.shape
    local, _, half = expert_gate.shape
    share = features // NT
    cap = rows // 2 * expert_ids.shape[1] // (local * NE // GROUPS)
    block = local * cap
    any_spec = pl.BlockSpec(memory_space=pl.ANY)
    vmem = pl.BlockSpec(memory_space=pltpu.VMEM)
    dma = pltpu.SemaphoreType.DMA
    return pl.pallas_call(
        kernel,
        out_shape=jax.ShapeDtypeStruct((rows, share), BF16),
        in_specs=[any_spec, vmem, vmem, vmem, vmem, any_spec, any_spec, any_spec],
        out_specs=vmem,
        scratch_shapes=[
            pltpu.VMEM((rows, features), BF16),
            pltpu.VMEM((2 * local, half, features), BF16),
            pltpu.VMEM((NE * block, share), BF16),
            pltpu.VMEM((NT, CHUNKS, PER * block, share), BF16),
            pltpu.VMEM((NT, local, half, share), BF16),
            pltpu.VMEM((NT, CHUNKS, PER * block, local * half), BF16),
            pltpu.VMEM((CHUNKS, PER * block, share), F32),
            pltpu.VMEM((NE, block, share), F32),
            pltpu.VMEM((rows, NE * block), F32),
            dma((4,)),
            dma,
            dma((CHUNKS,)),
            dma,
            dma((NT, CHUNKS)),
            dma,
            dma,
            dma,
            dma((NT, CHUNKS)),
            dma,
            dma,
        ],
        compiler_params=pltpu.CompilerParams(
            collective_id=0, has_side_effects=True, vmem_limit_bytes=56 * 2**20
        ),
    )(
        tokens,
        norm_gain.reshape(1, features),
        norm_shift.reshape(1, features),
        expert_ids.T,
        gate_weights.T,
        expert_gate.transpose(0, 2, 1),
        expert_up.transpose(0, 2, 1),
        expert_down,
    )


def solution(mesh):
    return jax.shard_map(
        per_device,
        mesh=mesh,
        in_specs=(
            P("ep", None),
            P(),
            P(),
            P("ep", None),
            P("ep", None),
            P("ep", None, "tp"),
            P("ep", None, "tp"),
            P("ep", "tp", None),
        ),
        out_specs=P("ep", "tp"),
        check_vma=False,
    )
```

time: 151 us -> 56.5 us (0.37)
  the two profiles are of different devices: /device:TPU:25 before, /device:TPU:1 now
where the time goes in v1:
time: 56.5 us; the launch traced here: 56.2 us
  Pallas kernels  54.9 us (97%)
  local copies, waits for them, and re-layouts  1.38 us (2%)
    pallas_call x1, Pallas kernels, per_device(): pl.pallas_call(kernel, out_shape=jax.ShapeDtypeStruct((rows, share), BF16...  54.9 us
    unnamed x1, local copies, waits for them, and re-layouts  1.38 us

profile of v1, /device:TPU:1, one launch (start us, length us, event | category | flops | bytes accessed | tf_op | source)
XLA Modules:
  0.0 56.2 jit_solution(16084225668486226919)
XLA Ops:
  0.0 54.9 %shard_map.82 = bf16[64,256]{1,0:T(8,128)(2,1)} custom-call(bf16[64,2048]{1,0:T(8,128)(2,1)} %tokens_h.1, f32[1,2048]{1,0:T(1,128)} %bitcast.8, f32[1,2048]{1,0:T(1,128)} %bitcast.9, s32[4,64]{1,0:T(4,128)} %bitcast.10, f32[4,64]{1,0:T(4,128)} %bitcast.11, bf16[2,64,2048]{2,1,0:T(8,128)(2,1)} %bitcast.6, bf16[2,64,2048]{2,1,0:T(8,128)(2,1)} %bitcast.7, ...), custom_call_target="tpu_custom_call" | custom-call | tf_op jit(solution)/shard_map/pallas_call | solution.py:242
  54.9 1.4 %copy.10 = bf16[64,256]{1,0:T(8,128)(2,1)} copy(bf16[64,256]{1,0:T(8,128)(2,1)} %shard_map.82) | data formatting | bytes 65536

commit v2 on v1

--- a/solution.py
+++ b/solution.py
@@ -14,6 +14,7 @@
 CHUNKS = 4
 PER = NE // CHUNKS
 epsilon = 1e-05
+LEVELS = 32767.0
 F32, BF16 = jnp.float32, jnp.bfloat16
 
 
@@ -25,8 +26,9 @@
 
 def kernel(
     tokens_h, gain_v, shift_v, ids_v, gw_v, gate_h, up_h, down_h, out_v,
-    tok, wall, packed, gath, wd, hid, outb, ret, combine,
+    tok, wall, packed, gath, wd, hid, outb, outs, ret, rets, combine,
     load_sem, disp_send, disp_recv, ag_send, ag_recv, wd_send, wd_recv, hid_send, hid_recv, ret_send, ret_recv,
+    rets_send, rets_recv,
 ):
     ep, tp = lax.axis_index("ep"), lax.axis_index("tp")
     ez, ex = ep // NX, ep % NX
@@ -88,9 +90,6 @@
     spread_f = jnp.where(spread, 1.0, 0.0)
     wanted = (lax.broadcasted_iota(jnp.int32, (slots, rows), 0) % cap + 1).astype(F32)
     place = jnp.dot(spread_f.astype(BF16), code, preferred_element_type=F32) == wanted
-    w_slots = jnp.dot(spread_f, weights, preferred_element_type=F32, precision=lax.Precision.HIGHEST)
-    combine[...] = jnp.where(place, w_slots, 0.0).T
-
     load_tok.wait()
     values = tok[...].astype(F32)
     centre = jnp.mean(values, axis=-1, keepdims=True)
@@ -101,7 +100,8 @@
     packed[...] = jnp.dot(jnp.where(place, 1.0, 0.0).astype(BF16), normed, preferred_element_type=F32).astype(BF16)
     gath[tp, 0, :block, :] = packed[pl.ds(pl.multiple_of(ep * block, block), block), :]
 
-    pl.semaphore_wait(barrier, NE - 1 + NT - 1)
+    with jax.named_scope("entry_wait"):
+        pl.semaphore_wait(barrier, NE - 1 + NT - 1)
 
     @pl.loop(1, NE)
     def _(n):
@@ -127,29 +127,25 @@
             device_id_type=MESH,
         ).start()
 
+    w_slots = jnp.dot(spread_f, weights, preferred_element_type=F32, precision=lax.Precision.HIGHEST)
+    combine[...] = jnp.where(place, w_slots, 0.0).T
+
     def arrived(ref, sem):
         pltpu.make_async_copy(ref, ref, sem).wait()
 
-    def share_out(buf, slot, q, send, recv, t):
+    def share_out(buf, slot, q, send, recv, t, part=None):
+        ref = buf.at[slot, q] if part is None else buf.at[slot, q, part]
         pltpu.make_async_remote_copy(
-            src_ref=buf.at[slot, q],
-            dst_ref=buf.at[slot, q],
+            src_ref=ref,
+            dst_ref=ref,
             send_sem=send,
             recv_sem=recv.at[slot, q],
             device_id=(ep, t),
             device_id_type=MESH,
         ).start()
 
-    def spread_own(buf, q, send, recv):
-        for dy in (2, 1, 3):
-            share_out(buf, tp, q, send, recv, ((ty + dy) % NY) * NC + tc)
-        share_out(buf, tp, q, send, recv, mate)
-
-    def forward(buf, q, send, recv):
-        for dy in (1, 3, 2):
-            slot = ((ty + dy) % NY) * NC + tc
-            arrived(buf.at[slot, q], recv.at[slot, q])
-            share_out(buf, slot, q, send, recv, mate)
+    def along(dy):
+        return ((ty + dy) % NY) * NC + tc
 
     def from_mate(buf, q, recv):
         for dy in (0, 1, 3, 2):
@@ -157,6 +153,8 @@
             arrived(buf.at[slot, q], recv.at[slot, q])
 
     chunk_rows = PER * block
+
+    halves = (pl.ds(0, chunk_rows // 2), pl.ds(chunk_rows // 2, chunk_rows // 2))
 
     def stage_a(q):
         if q == 0:
@@ -164,12 +162,21 @@
         else:
             part = gath.at[tp, q]
         arrived(part, disp_recv.at[q])
-        spread_own(gath, q, ag_send, ag_recv)
+        share_out(gath, tp, q, ag_send, ag_recv, along(1))
+        share_out(gath, tp, q, ag_send, ag_recv, along(3))
+        share_out(gath, tp, q, ag_send, ag_recv, mate)
 
     def stage_b(q):
-        forward(gath, q, ag_send, ag_recv)
+        for here, there, part in ((3, 1, halves[0]), (1, 3, halves[1])):
+            arrived(gath.at[along(here), q], ag_recv.at[along(here), q])
+            share_out(gath, along(here), q, ag_send, ag_recv, along(there), part)
+            share_out(gath, along(here), q, ag_send, ag_recv, mate)
 
     def stage_c(q):
+        arrived(gath.at[along(2), q], ag_recv.at[along(2), q])
+        share_out(gath, along(2), q, ag_send, ag_recv, mate)
+
+    def stage_d(q):
         if q == 0:
             load_gate.wait()
             load_up.wait()
@@ -179,25 +186,42 @@
             x, wall[...].reshape(4 * half, features), (((1,), (1,)), ((), ())), preferred_element_type=F32
         )
         g, u = both[:, : 2 * half], both[:, 2 * half :]
-        h = g / (1.0 + jnp.exp(-g)) * u
-        row = lax.broadcasted_iota(jnp.int32, h.shape, 0)
-        lane = lax.broadcasted_iota(jnp.int32, h.shape, 1)
-        hid[tp, q] = jnp.where((row % block) // cap == lane // half, h, 0.0).astype(BF16)
-        spread_own(hid, q, hid_send, hid_recv)
-
-    def stage_d(q):
-        forward(hid, q, hid_send, hid_recv)
+        h = (g / (1.0 + jnp.exp(-g)) * u).reshape(PER, 2, cap, 2 * half)
+        lane = lax.broadcasted_iota(jnp.int32, (PER, cap, 2 * half), 2)
+        h = jnp.where(lane < half, h[:, 0], h[:, 1])
+        hid[tp, q] = h.reshape(PER * cap, 2 * half).astype(BF16)
+        for dy in (2, 1, 3):
+            share_out(hid, tp, q, hid_send, hid_recv, along(dy))
+        share_out(hid, tp, q, hid_send, hid_recv, mate)
 
     def stage_e(q):
+        for dy in (1, 3, 2):
+            arrived(hid.at[along(dy), q], hid_recv.at[along(dy), q])
+            share_out(hid, along(dy), q, hid_send, hid_recv, mate)
+
+    def stage_f(q):
         if q == 0:
             load_down.wait()
             arrived(wd.at[pl.ds(0, NT - 1)], wd_recv)
         from_mate(hid, q, hid_recv)
-        x = jnp.concatenate([hid[s, q] for s in range(NT)], axis=-1)
+        lane = lax.broadcasted_iota(jnp.int32, (PER, cap, 2 * half), 2)
+        parts = []
+        for s in range(NT):
+            h = hid[s, q].astype(F32).reshape(PER, cap, 2 * half)
+            pair = jnp.stack([jnp.where(lane < half, h, 0.0), jnp.where(lane < half, 0.0, h)], axis=1)
+            parts.append(pair.reshape(chunk_rows, 2 * half).astype(BF16))
+        x = jnp.concatenate(parts, axis=-1)
         result = jnp.dot(x, wd[...].reshape(NT * 2 * half, share), preferred_element_type=F32)
-        outb[q] = result
+        top = jnp.maximum(jnp.max(jnp.abs(result), axis=-1, keepdims=True), 1e-30)
+        level = jnp.round(result * (LEVELS / top)).astype(jnp.int32)
+        outb[q] = level.astype(jnp.int16)
+        row = lax.broadcasted_iota(jnp.int32, (chunk_rows, 128), 0) % block
+        col = lax.broadcasted_iota(jnp.int32, (chunk_rows, 128), 1)
+        scales = jnp.where(col == row + (ep % (128 // block)) * block, top * (1.0 / LEVELS), 0.0)
+        outs[q] = jnp.sum(scales.reshape(PER, block, 128), axis=1, keepdims=True)
         if q == 0:
-            ret[ep] = result[:block]
+            ret[ep] = outb[0, 0:block]
+            rets[ep] = outs[0, 0]
 
         @pl.loop(1 if q == 0 else 0, PER)
         def _(r):
@@ -210,17 +234,30 @@
                 device_id=(dest, tp),
                 device_id_type=MESH,
             ).start()
-
-    stages = (stage_a, stage_b, stage_c, stage_d, stage_e)
+            pltpu.make_async_remote_copy(
+                src_ref=outs.at[q, r],
+                dst_ref=rets.at[ep],
+                send_sem=rets_send,
+                recv_sem=rets_recv,
+                device_id=(dest, tp),
+                device_id_type=MESH,
+            ).start()
+
+    stages = (stage_a, stage_b, stage_c, stage_d, stage_e, stage_f)
     for step in range(CHUNKS + len(stages) - 1):
         for lag, stage in enumerate(stages):
             if 0 <= step - lag < CHUNKS:
-                stage(step - lag)
-
-    arrived(ret.at[pl.ds(0, NE - 1)], ret_recv)
-    back = ret[...].reshape(NE * block, share)
+                with jax.named_scope(f"{stage.__name__}{step - lag}"):
+                    stage(step - lag)
+
+    with jax.named_scope("ret_wait"):
+        arrived(ret.at[pl.ds(0, NE - 1)], ret_recv)
+    arrived(rets.at[pl.ds(0, NE - 1)], rets_recv)
+    per = 128 // block
+    scale = jnp.concatenate([jnp.sum(rets[pl.ds(i * per, per)], axis=0) for i in range(NE // per)], axis=-1)
+    back = ret[...].astype(jnp.int32).astype(F32).reshape(NE * block, share)
     out_v[...] = jnp.dot(
-        combine[...], back, preferred_element_type=F32, precision=lax.Precision.HIGHEST
+        combine[...] * scale, back, preferred_element_type=F32, precision=lax.Precision.HIGHEST
     ).astype(BF16)
 
     arrived(packed.at[pl.ds(0, (NE - 1) * block)], disp_send)
@@ -228,6 +265,7 @@
     arrived(gath.at[pl.ds(0, NT - 1)], ag_send)
     arrived(hid.at[pl.ds(0, NT - 1)], hid_send)
     arrived(ret.at[pl.ds(0, NE - 1)], ret_send)
+    arrived(rets.at[pl.ds(0, NE - 1)], rets_send)
 
 
 def per_device(tokens, norm_gain, norm_shift, expert_ids, gate_weights, expert_gate, expert_up, expert_down):
@@ -250,9 +288,11 @@
             pltpu.VMEM((NE * block, share), BF16),
             pltpu.VMEM((NT, CHUNKS, PER * block, share), BF16),
             pltpu.VMEM((NT, local, half, share), BF16),
-            pltpu.VMEM((NT, CHUNKS, PER * block, local * half), BF16),
-            pltpu.VMEM((CHUNKS, PER * block, share), F32),
-            pltpu.VMEM((NE, block, share), F32),
+            pltpu.VMEM((NT, CHUNKS, PER * cap, local * half), BF16),
+            pltpu.VMEM((CHUNKS, PER * block, share), jnp.int16),
+            pltpu.VMEM((CHUNKS, PER, 1, 128), F32),
+            pltpu.VMEM((NE, block, share), jnp.int16),
+            pltpu.VMEM((NE, 1, 128), F32),
             pltpu.VMEM((rows, NE * block), F32),
             dma((4,)),
             dma,
@@ -263,6 +303,8 @@
             dma,
             dma,
             dma((NT, CHUNKS)),
+            dma,
+            dma,
             dma,
             dma,
         ],

time: 56.5 us -> 54.2 us (0.959)
  Pallas kernels: 54.9 us -> 52.7 us
    pallas_call x1, Pallas kernels: 54.9 us -> 52.7 us  [per_device(): pl.pallas_call(kernel, out_shape=jax.ShapeDtypeStruct((rows, share), BF16...]
where the time goes in v2:
time: 54.2 us; the launch traced here: 54 us
  Pallas kernels  52.7 us (97%)
  local copies, waits for them, and re-layouts  1.38 us (3%)
    pallas_call x1, Pallas kernels, per_device(): pl.pallas_call(kernel, out_shape=jax.ShapeDtypeStruct((rows, share), BF16...  52.7 us
    unnamed x1, local copies, waits for them, and re-layouts  1.38 us

profile of v2, /device:TPU:1, one launch (start us, length us, event | category | flops | bytes accessed | tf_op | source)
XLA Modules:
  0.0 54.0 jit_solution(1156918163298414972)
XLA Ops:
  0.0 52.7 %shard_map.82 = bf16[64,256]{1,0:T(8,128)(2,1)} custom-call(bf16[64,2048]{1,0:T(8,128)(2,1)} %tokens_h.1, f32[1,2048]{1,0:T(1,128)} %bitcast.8, f32[1,2048]{1,0:T(1,128)} %bitcast.9, s32[4,64]{1,0:T(4,128)} %bitcast.10, f32[4,64]{1,0:T(4,128)} %bitcast.11, bf16[2,64,2048]{2,1,0:T(8,128)(2,1)} %bitcast.6, bf16[2,64,2048]{2,1,0:T(8,128)(2,1)} %bitcast.7, ...), custom_call_target="tpu_custom_call" | custom-call | tf_op jit(solution)/shard_map/pallas_call | solution.py:280
  52.7 1.4 %copy.10 = bf16[64,256]{1,0:T(8,128)(2,1)} copy(bf16[64,256]{1,0:T(8,128)(2,1)} %shard_map.82) | data formatting | bytes 65536

commit v3 on v0

v3 whole, which is shorter than its diff:
```python
import jax
import jax.numpy as jnp
from jax import lax
from jax.experimental import pallas as pl
from jax.experimental.pallas import tpu as pltpu
from jax.sharding import PartitionSpec as P

MESH = pl.DeviceIdType.MESH
GROUPS = 4
NZ, NX, NY, NC = 8, 4, 4, 2
NE, NT = NZ * NX, NY * NC
ABSOLUTE = 2
SEND_FAR = True
SIG_FAR = True
ORDER = (0, 7, 1, 6, 2, 5, 3, 4)
CHUNKS = 4
LINES = NZ // CHUNKS
PER = NE // CHUNKS
RELAY = True
SEQ = ("a0", "a1", "a2", "a3", "b0", "b1", "b2", "b3", "d0", "d1", "d2", "d3", "f0", "f1", "f2", "f3")
FINAL_CAST = True
VMEM_LIMIT = 56 * 2**20
epsilon = 1e-05
LEVELS = 32767.0
F32, BF16 = jnp.float32, jnp.bfloat16


def kernel(
    tokens_h, gain_v, shift_v, ids_v, gw_v, gate_h, up_h, down_h, out_v,
    tok, wall, packed, gath, wd, hid, outb, outs, ret, rets, combine,
    load_sem, disp_send, disp_recv, ag_send, ag_recv, wall_send, wall_recv, wd_send, wd_recv, hid_send, hid_recv,
    ret_send, ret_recv, rets_send, rets_recv,
):
    ep, tp = lax.axis_index("ep"), lax.axis_index("tp")
    ez, ex = ep // NX, ep % NX
    ty, tc = tp // NC, tp % NC
    mate = ty * NC + 1 - tc
    rows, features = tok.shape
    quarter = features // NY
    share = quarter // NC
    block = packed.shape[0] // NE
    cap = block // NC
    half = wall.shape[2]
    chunk_rows = PER * block
    work_rows = PER * cap
    own_line = (ORDER.index(0), ez, ez % 4 * 2 + ez // 4, ez // 4 * 4 + ez % 2 * 2 + ez % 4 // 2)[ABSOLUTE]
    own_q = own_line // LINES

    def arrived(ref, sem):
        pltpu.make_async_copy(ref, ref, sem).wait()

    def send(src, dst, send_sem, recv_sem, e, t):
        pltpu.make_async_remote_copy(
            src_ref=src, dst_ref=dst, send_sem=send_sem, recv_sem=recv_sem, device_id=(e, t), device_id_type=MESH
        ).start()

    def rows_of(n):
        return pl.ds(pl.multiple_of(n * block, block), block)

    def quarter_of(y):
        return pl.ds(pl.multiple_of(y * quarter, quarter), quarter)

    load_tok = pltpu.make_async_copy(tokens_h, tok, load_sem.at[0])
    load_gate = pltpu.make_async_copy(gate_h.at[tc], wall.at[0, tc], load_sem.at[1])
    load_up = pltpu.make_async_copy(up_h.at[tc], wall.at[1, tc], load_sem.at[2])
    load_down = pltpu.make_async_copy(down_h.at[tc, :, quarter_of(ty)], wd.at[tp], load_sem.at[3])
    load_tok.start()

    barrier = pltpu.get_barrier_semaphore()

    def signal(e, t):
        pl.semaphore_signal(barrier, inc=1, device_id=(e, t), device_id_type=MESH)

    for dz in (4, 3, 5, 2, 6, 1, 7, 0):
        for dx in range(1 if dz == 0 else 0, NX):
            signal(((ez + dz) % NZ) * NX + (ex + dx) % NX, tp)
    for d in range(1, NT):
        signal(ep, (tp + d) % NT)

    ids, gw = ids_v[...], gw_v[...]
    earlier = lax.broadcasted_iota(jnp.int32, (rows, rows), 0) < lax.broadcasted_iota(jnp.int32, (rows, rows), 1)
    earlier = jnp.where(earlier, 1.0, 0.0).astype(BF16)

    def placed(numbers):
        hits = jnp.zeros(numbers.shape, F32)
        weights = jnp.zeros(numbers.shape, F32)
        for k in range(ids.shape[0]):
            same = ids[k : k + 1, :] == numbers
            hits = hits + jnp.where(same, 1.0, 0.0)
            weights = weights + jnp.where(same, gw[k : k + 1, :], 0.0)
        before = jnp.dot(hits.astype(BF16), earlier, preferred_element_type=F32)
        code = hits * (before + 1.0)
        wanted = (lax.broadcasted_iota(jnp.int32, (numbers.shape[0], cap, rows), 1) + 1).astype(F32)
        return code[:, None, :] == wanted, weights

    with jax.named_scope("p_place"):
        place, _ = placed(lax.broadcasted_iota(jnp.int32, (NE, rows), 0) * NC + tc)
        place = jnp.where(place, 1.0, 0.0).reshape(NE * cap, rows).astype(BF16)

    load_tok.wait()
    load_gate.start()
    load_up.start()
    load_down.start()
    with jax.named_scope("p_ln"):
        values = tok[...].astype(F32)
        centre = jnp.mean(values, axis=-1, keepdims=True)
        spread = jnp.mean(jnp.square(values - centre), axis=-1, keepdims=True)
        own = tok[:, quarter_of(ty)].astype(F32)
        normed = (own - centre) * lax.rsqrt(spread + epsilon) * gain_v[:, quarter_of(ty)] + shift_v[:, quarter_of(ty)]
        picked = jnp.dot(place, normed.astype(BF16), preferred_element_type=F32).reshape(NE, cap, quarter)
        picked = jnp.stack([picked[:, :, :share], picked[:, :, share:]], axis=1)
        packed[...] = picked.reshape(NE * block, share).astype(BF16)
        gath[ty, own_q, rows_of(own_line % LINES * NX + ex), :] = packed[rows_of(ep), :]

    with jax.named_scope("entry_wait"):
        pl.semaphore_wait(barrier, NE - 1 + NT - 1)

    sends = tuple(enumerate(ORDER))
    for line, dz in reversed(sends) if SEND_FAR else sends:
        line = own_line if ABSOLUTE else line

        @pl.loop(1 if dz == 0 else 0, NX)
        def _(dx):
            e = ((ez + NZ - dz) % NZ) * NX + (ex + dx) % NX
            send(
                packed.at[rows_of(e)], gath.at[ty, line // LINES, rows_of(line % LINES * NX + ex)],
                disp_send, disp_recv.at[line // LINES], e, tp,
            )

    for d in range(1, NT):
        t = (tp + d) % NT
        send(down_h.at[t % NC, :, quarter_of(t // NC)], wd.at[tp], wd_send, wd_recv, ep, t)

    send(gate_h.at[1 - tc], wall.at[0, tc], wall_send, wall_recv, ep, mate)
    send(up_h.at[1 - tc], wall.at[1, tc], wall_send, wall_recv, ep, mate)

    with jax.named_scope("p_combine"):
        place, weights = placed(lax.broadcasted_iota(jnp.int32, (NE * NC, rows), 0))
        w_slots = jnp.where(place, weights[:, None, :], 0.0).reshape(NE * block, rows)
        combine[...] = w_slots.T

    def share_out(buf, y, q, send_sem, recv_sem, to, part=None):
        ref = buf.at[y, q] if part is None else buf.at[y, q, part]
        send(ref, ref, send_sem, recv_sem, ep, to * NC + tc)

    def along(dy):
        return (ty + dy) % NY

    halves = (pl.ds(0, chunk_rows // 2), pl.ds(chunk_rows // 2, chunk_rows // 2))

    def stage_a(q):
        @pl.when(own_q == q)
        def _():
            arrived(gath.at[ty, q, pl.ds(0, chunk_rows - block)], disp_recv.at[q])

        @pl.when(own_q != q)
        def _():
            arrived(gath.at[ty, q], disp_recv.at[q])

        if not RELAY:
            share_out(gath, ty, q, ag_send, ag_recv.at[ty, q], along(2))
        share_out(gath, ty, q, ag_send, ag_recv.at[ty, q], along(1))
        share_out(gath, ty, q, ag_send, ag_recv.at[ty, q], along(3))

    def stage_b(q):
        for here, there, part in ((3, 1, halves[0]), (1, 3, halves[1])):
            arrived(gath.at[along(here), q], ag_recv.at[along(here), q])
            if RELAY:
                share_out(gath, along(here), q, ag_send, ag_recv.at[along(here), q], along(there), part)

    def stage_d(q):
        if q == 0:
            load_gate.wait()
            load_up.wait()
            arrived(wall.at[0], wall_recv)
        arrived(gath.at[along(2), q], ag_recv.at[along(2), q])
        parts = []
        for y in range(NY):
            both = gath[y, q].astype(F32).reshape(PER, NC, cap, share)
            parts += [both[:, i].reshape(work_rows, share).astype(BF16) for i in range(NC)]
        x = jnp.concatenate(parts, axis=-1)
        both = lax.dot_general(
            x, wall[...].reshape(2 * NC * half, features), (((1,), (1,)), ((), ())), preferred_element_type=F32
        )
        g, u = both[:, : NC * half], both[:, NC * half :]
        hid[ty, q] = (g / (1.0 + jnp.exp(-g)) * u).astype(BF16)
        for dy in (2, 1, 3):
            share_out(hid, ty, q, hid_send, hid_recv.at[q], along(dy))

    def stage_f(q):
        if q == 0:
            load_down.wait()
            arrived(wd.at[pl.ds(0, NT - 1)], wd_recv)
        arrived(hid.at[pl.ds(0, NY - 1), q], hid_recv.at[q])
        x = jnp.concatenate([hid[y, q] for y in range(NY)], axis=-1)
        result = jnp.dot(x, wd[...].reshape(NT * half, quarter), preferred_element_type=F32)
        top = jnp.maximum(jnp.max(jnp.abs(result), axis=-1, keepdims=True), 1e-30)
        level = jnp.round(result * (LEVELS / top)).astype(jnp.int32)
        tiles = [level[:, i : i + 128].reshape(PER, cap, 128) for i in range(0, quarter, 128)]
        outb[q] = jnp.stack(tiles, axis=1).reshape(PER, NC, block, 128).astype(jnp.int16)
        row = lax.broadcasted_iota(jnp.int32, (work_rows, 128), 0) % cap
        col = lax.broadcasted_iota(jnp.int32, (work_rows, 128), 1)
        scales = jnp.where(col == row + tc * cap + ep % (128 // block) * block, top * (1.0 / LEVELS), 0.0)
        outs[q] = jnp.sum(scales.reshape(PER, cap, 128), axis=1, keepdims=True)

        @pl.when(own_q == q)
        def _():
            r = own_line % LINES * NX + ex
            ret[ep * NC + tc] = outb[q, r, tc]
            rets[ep * NC + tc] = outs[q, r]

        for k in range(LINES):
            line = q * LINES + k
            z = ((ez + ORDER[line]) % NZ, line, line // 2 + line % 2 * 4, line // 4 * 4 + line % 2 * 2 + line % 4 // 2)[ABSOLUTE]

            @pl.loop(0, NX)
            def _(x):
                e, r = z * NX + x, k * NX + x
                for c in range(NC):

                    @pl.when((e != ep) | (c != tc))
                    def _():
                        t = ty * NC + c
                        send(outb.at[q, r, c], ret.at[ep * NC + tc], ret_send, ret_recv, e, t)
                        send(outs.at[q, r], rets.at[ep * NC + tc], rets_send, rets_recv, e, t)

    stages = {"a": stage_a, "b": stage_b, "d": stage_d, "f": stage_f}
    for word in SEQ:
        with jax.named_scope(f"stage_{word}"):
            stages[word[0]](int(word[1:]))

    with jax.named_scope("ret_wait"):
        arrived(ret.at[pl.ds(0, NE * NC - 1)], ret_recv)
        arrived(rets.at[pl.ds(0, NE * NC - 1)], rets_recv)
    per = 128 // block
    scale = jnp.concatenate(
        [jnp.sum(rets[pl.ds(i * per * NC, per * NC)], axis=0) for i in range(NE // per)], axis=-1
    )
    back = ret[...].astype(jnp.int32).astype(F32).reshape(NE, NC, share // 128, cap, 128)
    back = jnp.concatenate([back[:, :, i].reshape(NE * block, 128) for i in range(share // 128)], axis=-1)
    out_v[...] = jnp.dot(
        combine[...] * scale, back, preferred_element_type=F32, precision=lax.Precision.HIGHEST
    ).astype(out_v.dtype)

    with jax.named_scope("drain"):
        arrived(packed.at[pl.ds(0, (NE - 1) * block)], disp_send)
        arrived(wd.at[pl.ds(0, NT - 1)], wd_send)
        arrived(wall.at[0], wall_send)
        arrived(gath.at[pl.ds(0, NY - 1)], ag_send)
        arrived(hid.at[pl.ds(0, NY - 1)], hid_send)
        arrived(ret.at[pl.ds(0, NE * NC - 1)], ret_send)
        arrived(rets.at[pl.ds(0, NE * NC - 1)], rets_send)


def per_device(tokens, norm_gain, norm_shift, expert_ids, gate_weights, expert_gate, expert_up, expert_down):
    rows, features = tokens.shape
    local, _, half = expert_gate.shape
    quarter = features // NY
    share = features // NT
    cap = rows // 2 * expert_ids.shape[1] // (local * NE // GROUPS)
    block = local * cap
    any_spec = pl.BlockSpec(memory_space=pl.ANY)
    vmem = pl.BlockSpec(memory_space=pltpu.VMEM)
    dma = pltpu.SemaphoreType.DMA
    out = pl.pallas_call(
        kernel,
        out_shape=jax.ShapeDtypeStruct((rows, share), F32 if FINAL_CAST else BF16),
        in_specs=[any_spec, vmem, vmem, vmem, vmem, any_spec, any_spec, any_spec],
        out_specs=vmem,
        scratch_shapes=[
            pltpu.VMEM((rows, features), BF16),
            pltpu.VMEM((2, NC, half, features), BF16),
            pltpu.VMEM((NE * block, share), BF16),
            pltpu.VMEM((NY, CHUNKS, PER * block, share), BF16),
            pltpu.VMEM((NT, half, quarter), BF16),
            pltpu.VMEM((NY, CHUNKS, PER * cap, NC * half), BF16),
            pltpu.VMEM((CHUNKS, PER, NC, block, 128), jnp.int16),
            pltpu.VMEM((CHUNKS, PER, 1, 128), F32),
            pltpu.VMEM((NE * NC, block, 128), jnp.int16),
            pltpu.VMEM((NE * NC, 1, 128), F32),
            pltpu.VMEM((rows, NE * block), F32),
            dma((4,)),
            dma,
            dma((CHUNKS,)),
            dma,
            dma((NY, CHUNKS)),
            dma,
            dma,
            dma,
            dma,
            dma,
            dma((CHUNKS,)),
            dma,
            dma,
            dma,
            dma,
        ],
        compiler_params=pltpu.CompilerParams(collective_id=0, has_side_effects=True, vmem_limit_bytes=VMEM_LIMIT),
    )(
        tokens,
        norm_gain.reshape(1, features),
        norm_shift.reshape(1, features),
        expert_ids.T,
        gate_weights.T,
        expert_gate.transpose(0, 2, 1),
        expert_up.transpose(0, 2, 1),
        expert_down,
    )
    return out.astype(BF16)


def solution(mesh):
    return jax.shard_map(
        per_device,
        mesh=mesh,
        in_specs=(
            P("ep", None),
            P(),
            P(),
            P("ep", None),
            P("ep", None),
            P("ep", None, "tp"),
            P("ep", None, "tp"),
            P("ep", "tp", None),
        ),
        out_specs=P("ep", "tp"),
        check_vma=False,
    )
```

time: 151 us -> 45.3 us (0.30)
  the two profiles are of different devices: /device:TPU:25 before, /device:TPU:1 now
where the time goes in v3:
time: 45.3 us; the launch traced here: 45 us
  Pallas kernels  43.5 us (96%)
  other arithmetic  1.46 us (3%)
    pallas_call x1, Pallas kernels, per_device(): pl.pallas_call(kernel, out_shape=jax.ShapeDtypeStruct((rows, share), F32...  43.5 us
    convert_element_type x1, other arithmetic, per_device(): return out.astype(BF16)  1.46 us

profile of v3, /device:TPU:1, one launch (start us, length us, event | category | flops | bytes accessed | tf_op | source)
XLA Modules:
  0.0 45.0 jit_solution(7439672123728748657)
XLA Ops:
  0.0 43.5 %shard_map.82 = f32[64,256]{1,0:T(8,128)} custom-call(bf16[64,2048]{1,0:T(8,128)(2,1)} %tokens_h.1, f32[1,2048]{1,0:T(1,128)} %bitcast.8, f32[1,2048]{1,0:T(1,128)} %bitcast.9, s32[4,64]{1,0:T(4,128)} %bitcast.10, f32[4,64]{1,0:T(4,128)} %bitcast.11, bf16[2,64,2048]{2,1,0:T(8,128)(2,1)} %bitcast.6, bf16[2,64,2048]{2,1,0:T(8,128)(2,1)} %bitcast.7, ...), custom_call_target="tpu_custom_call" | custom-call | tf_op jit(solution)/shard_map/pallas_call | solution.py:265
  43.5 1.5 %convert_element_type.3 = bf16[64,256]{1,0:T(8,128)(2,1)} convert(f32[64,256]{1,0:T(8,128)} %shard_map.82) | non-fusion elementwise | flops 16384 | bytes 98304 | tf_op jit(solution)/shard_map/convert_element_type | solution.py:309

commit v4 on v3

--- a/solution.py
+++ b/solution.py
@@ -9,7 +9,8 @@
 GROUPS = 4
 NZ, NX, NY, NC = 8, 4, 4, 2
 NE, NT = NZ * NX, NY * NC
-ABSOLUTE = 2
+ABSOLUTE = True
+ZORDER = (0, 1, 2, 3, 4, 5, 6, 7)
 SEND_FAR = True
 SIG_FAR = True
 ORDER = (0, 7, 1, 6, 2, 5, 3, 4)
@@ -21,15 +22,16 @@
 FINAL_CAST = True
 VMEM_LIMIT = 56 * 2**20
 epsilon = 1e-05
-LEVELS = 32767.0
+LEVELS = 32760.0
+KEYS = 128.0
 F32, BF16 = jnp.float32, jnp.bfloat16
 
 
 def kernel(
     tokens_h, gain_v, shift_v, ids_v, gw_v, gate_h, up_h, down_h, out_v,
-    tok, wall, packed, gath, wd, hid, outb, outs, ret, rets, combine,
+    tok, wall, packed, gath, wd, hid, outb, ret, combine,
     load_sem, disp_send, disp_recv, ag_send, ag_recv, wall_send, wall_recv, wd_send, wd_recv, hid_send, hid_recv,
-    ret_send, ret_recv, rets_send, rets_recv,
+    ret_send, ret_recv,
 ):
     ep, tp = lax.axis_index("ep"), lax.axis_index("tp")
     ez, ex = ep // NX, ep % NX
@@ -43,7 +45,7 @@
     half = wall.shape[2]
     chunk_rows = PER * block
     work_rows = PER * cap
-    own_line = (ORDER.index(0), ez, ez % 4 * 2 + ez // 4, ez // 4 * 4 + ez % 2 * 2 + ez % 4 // 2)[ABSOLUTE]
+    own_line = sum(jnp.where(ez == z, line, 0) for line, z in enumerate(ZORDER)) if ABSOLUTE else ORDER.index(0)
     own_q = own_line // LINES
 
     def arrived(ref, sem):
@@ -195,23 +197,27 @@
         x = jnp.concatenate([hid[y, q] for y in range(NY)], axis=-1)
         result = jnp.dot(x, wd[...].reshape(NT * half, quarter), preferred_element_type=F32)
         top = jnp.maximum(jnp.max(jnp.abs(result), axis=-1, keepdims=True), 1e-30)
-        level = jnp.round(result * (LEVELS / top)).astype(jnp.int32)
-        tiles = [level[:, i : i + 128].reshape(PER, cap, 128) for i in range(0, quarter, 128)]
-        outb[q] = jnp.stack(tiles, axis=1).reshape(PER, NC, block, 128).astype(jnp.int16)
+        key = jnp.ceil(jnp.log2(top) * KEYS) + 1.0
+        level = jnp.round(result * (LEVELS * jnp.exp2(key * (-1.0 / KEYS)))).astype(jnp.int32)
+        for c in range(NC):
+            left = level[:, c * share : c * share + 128]
+            right = level[:, c * share + 128 : (c + 1) * share]
+            outb[q, :, c, 0:cap, :] = ((left << 16) | (right & 0xFFFF)).reshape(PER, cap, 128)
         row = lax.broadcasted_iota(jnp.int32, (work_rows, 128), 0) % cap
         col = lax.broadcasted_iota(jnp.int32, (work_rows, 128), 1)
-        scales = jnp.where(col == row + tc * cap + ep % (128 // block) * block, top * (1.0 / LEVELS), 0.0)
-        outs[q] = jnp.sum(scales.reshape(PER, cap, 128), axis=1, keepdims=True)
+        keys = jnp.where(col == row + tc * cap + ep % (128 // block) * block, key, 0.0)
+        keys = jnp.sum(keys.reshape(PER, cap, 128), axis=1, keepdims=True).astype(jnp.int32)
+        for c in range(NC):
+            outb[q, :, c, cap : cap + 1, :] = keys
 
         @pl.when(own_q == q)
         def _():
             r = own_line % LINES * NX + ex
             ret[ep * NC + tc] = outb[q, r, tc]
-            rets[ep * NC + tc] = outs[q, r]
 
         for k in range(LINES):
             line = q * LINES + k
-            z = ((ez + ORDER[line]) % NZ, line, line // 2 + line % 2 * 4, line // 4 * 4 + line % 2 * 2 + line % 4 // 2)[ABSOLUTE]
+            z = ZORDER[line] if ABSOLUTE else (ez + ORDER[line]) % NZ
 
             @pl.loop(0, NX)
             def _(x):
@@ -222,7 +228,6 @@
                     def _():
                         t = ty * NC + c
                         send(outb.at[q, r, c], ret.at[ep * NC + tc], ret_send, ret_recv, e, t)
-                        send(outs.at[q, r], rets.at[ep * NC + tc], rets_send, rets_recv, e, t)
 
     stages = {"a": stage_a, "b": stage_b, "d": stage_d, "f": stage_f}
     for word in SEQ:
@@ -231,13 +236,14 @@
 
     with jax.named_scope("ret_wait"):
         arrived(ret.at[pl.ds(0, NE * NC - 1)], ret_recv)
-        arrived(rets.at[pl.ds(0, NE * NC - 1)], rets_recv)
     per = 128 // block
-    scale = jnp.concatenate(
-        [jnp.sum(rets[pl.ds(i * per * NC, per * NC)], axis=0) for i in range(NE // per)], axis=-1
+    words = ret[:, 0:cap, :].reshape(NE * block, 128)
+    back = jnp.concatenate([words >> 16, (words << 16) >> 16], axis=-1).astype(F32)
+    keys = ret[:, cap : cap + 1, :].astype(F32)
+    keys = jnp.concatenate(
+        [jnp.sum(keys[i * per * NC : (i + 1) * per * NC], axis=0) for i in range(NE // per)], axis=-1
     )
-    back = ret[...].astype(jnp.int32).astype(F32).reshape(NE, NC, share // 128, cap, 128)
-    back = jnp.concatenate([back[:, :, i].reshape(NE * block, 128) for i in range(share // 128)], axis=-1)
+    scale = jnp.exp2(keys * (1.0 / KEYS)) * (1.0 / LEVELS)
     out_v[...] = jnp.dot(
         combine[...] * scale, back, preferred_element_type=F32, precision=lax.Precision.HIGHEST
     ).astype(out_v.dtype)
@@ -249,7 +255,6 @@
         arrived(gath.at[pl.ds(0, NY - 1)], ag_send)
         arrived(hid.at[pl.ds(0, NY - 1)], hid_send)
         arrived(ret.at[pl.ds(0, NE * NC - 1)], ret_send)
-        arrived(rets.at[pl.ds(0, NE * NC - 1)], rets_send)
 
 
 def per_device(tokens, norm_gain, norm_shift, expert_ids, gate_weights, expert_gate, expert_up, expert_down):
@@ -264,7 +269,7 @@
     dma = pltpu.SemaphoreType.DMA
     out = pl.pallas_call(
         kernel,
-        out_shape=jax.ShapeDtypeStruct((rows, share), F32 if FINAL_CAST else BF16),
+        out_shape=pltpu.VMEM((rows, share), F32),
         in_specs=[any_spec, vmem, vmem, vmem, vmem, any_spec, any_spec, any_spec],
         out_specs=vmem,
         scratch_shapes=[
@@ -274,10 +279,8 @@
             pltpu.VMEM((NY, CHUNKS, PER * block, share), BF16),
             pltpu.VMEM((NT, half, quarter), BF16),
             pltpu.VMEM((NY, CHUNKS, PER * cap, NC * half), BF16),
-            pltpu.VMEM((CHUNKS, PER, NC, block, 128), jnp.int16),
-            pltpu.VMEM((CHUNKS, PER, 1, 128), F32),
-            pltpu.VMEM((NE * NC, block, 128), jnp.int16),
-            pltpu.VMEM((NE * NC, 1, 128), F32),
+            pltpu.VMEM((CHUNKS, PER, NC, cap + 1, 128), jnp.int32),
+            pltpu.VMEM((NE * NC, cap + 1, 128), jnp.int32),
             pltpu.VMEM((rows, NE * block), F32),
             dma((4,)),
             dma,
@@ -290,8 +293,6 @@
             dma,
             dma,
             dma((CHUNKS,)),
-            dma,
-            dma,
             dma,
             dma,
         ],

time: 45.3 us -> 42.2 us (0.932)
  Pallas kernels: 43.5 us -> 41.1 us
  other arithmetic: 1.46 us -> 0.62 us
    pallas_call x1, Pallas kernels: 43.5 us -> 41.1 us  [per_device(): pl.pallas_call(kernel, out_shape=pltpu.VMEM((rows, share), F32), in_specs...]
    convert_element_type x1, other arithmetic: 1.46 us -> 0.62 us  [per_device(): return out.astype(BF16)]
where the time goes in v4:
time: 42.2 us; the launch traced here: 41.7 us
  Pallas kernels  41.1 us (97%)
  other arithmetic  0.62 us (1%)
    pallas_call x1, Pallas kernels, per_device(): pl.pallas_call(kernel, out_shape=pltpu.VMEM((rows, share), F32), in_specs...  41.1 us

profile of v4, /device:TPU:1, one launch (start us, length us, event | category | flops | bytes accessed | tf_op | source)
XLA Modules:
  0.0 41.7 jit_solution(2204643094484399303)
XLA Ops:
  0.0 41.1 %shard_map.82 = f32[64,256]{1,0:T(8,128)S(1)} custom-call(bf16[64,2048]{1,0:T(8,128)(2,1)} %tokens_h.1, f32[1,2048]{1,0:T(1,128)} %bitcast.8, f32[1,2048]{1,0:T(1,128)} %bitcast.9, s32[4,64]{1,0:T(4,128)} %bitcast.10, f32[4,64]{1,0:T(4,128)} %bitcast.11, bf16[2,64,2048]{2,1,0:T(8,128)(2,1)} %bitcast.6, bf16[2,64,2048]{2,1,0:T(8,128)(2,1)} %bitcast.7, ...), custom_call_target="tpu_custom_call" | custom-call | tf_op jit(solution)/shard_map/pallas_call | solution.py:270
  41.1 0.6 %convert_element_type.3 = bf16[64,256]{1,0:T(8,128)(2,1)} convert(f32[64,256]{1,0:T(8,128)S(1)} %shard_map.82) | non-fusion elementwise | flops 16384 | bytes 98304 | tf_op jit(solution)/shard_map/convert_element_type | solution.py:310

commit v5 on v4

--- a/solution.py
+++ b/solution.py
@@ -17,8 +17,8 @@
 CHUNKS = 4
 LINES = NZ // CHUNKS
 PER = NE // CHUNKS
-RELAY = True
-SEQ = ("a0", "a1", "a2", "a3", "b0", "b1", "b2", "b3", "d0", "d1", "d2", "d3", "f0", "f1", "f2", "f3")
+FAR_AT = 0
+SEQ = ("a0", "a1", "a2", "a3", "d0", "d1", "d2", "d3", "f0", "f1", "f2", "f3")
 FINAL_CAST = True
 VMEM_LIMIT = 56 * 2**20
 epsilon = 1e-05
@@ -29,8 +29,8 @@
 
 def kernel(
     tokens_h, gain_v, shift_v, ids_v, gw_v, gate_h, up_h, down_h, out_v,
-    tok, wall, packed, gath, wd, hid, outb, ret, combine,
-    load_sem, disp_send, disp_recv, ag_send, ag_recv, wall_send, wall_recv, wd_send, wd_recv, hid_send, hid_recv,
+    tok, wall, columns, packed, spare, gath, wd, hid, outb, ret, combine,
+    load_sem, disp_send, disp_recv, far_send, far_recv, ag_send, ag_recv, wall_send, wall_recv, wd_send, wd_recv, hid_send, hid_recv,
     ret_send, ret_recv,
 ):
     ep, tp = lax.axis_index("ep"), lax.axis_index("tp")
@@ -107,27 +107,35 @@
         values = tok[...].astype(F32)
         centre = jnp.mean(values, axis=-1, keepdims=True)
         spread = jnp.mean(jnp.square(values - centre), axis=-1, keepdims=True)
-        own = tok[:, quarter_of(ty)].astype(F32)
-        normed = (own - centre) * lax.rsqrt(spread + epsilon) * gain_v[:, quarter_of(ty)] + shift_v[:, quarter_of(ty)]
-        picked = jnp.dot(place, normed.astype(BF16), preferred_element_type=F32).reshape(NE, cap, quarter)
-        picked = jnp.stack([picked[:, :, :share], picked[:, :, share:]], axis=1)
-        packed[...] = picked.reshape(NE * block, share).astype(BF16)
-        gath[ty, own_q, rows_of(own_line % LINES * NX + ex), :] = packed[rows_of(ep), :]
+        scale = lax.rsqrt(spread + epsilon)
+
+        def pack(y, buf):
+            own = tok[:, quarter_of(y)].astype(F32)
+            normed = (own - centre) * scale * gain_v[:, quarter_of(y)] + shift_v[:, quarter_of(y)]
+            picked = jnp.dot(place, normed.astype(BF16), preferred_element_type=F32).reshape(NE, cap, quarter)
+            picked = jnp.stack([picked[:, :, :share], picked[:, :, share:]], axis=1)
+            buf[...] = picked.reshape(NE * block, share).astype(BF16)
+            gath[y, own_q, rows_of(own_line % LINES * NX + ex), :] = buf[rows_of(ep), :]
+
+        pack(ty, packed)
 
     with jax.named_scope("entry_wait"):
         pl.semaphore_wait(barrier, NE - 1 + NT - 1)
 
-    sends = tuple(enumerate(ORDER))
-    for line, dz in reversed(sends) if SEND_FAR else sends:
-        line = own_line if ABSOLUTE else line
-
-        @pl.loop(1 if dz == 0 else 0, NX)
-        def _(dx):
-            e = ((ez + NZ - dz) % NZ) * NX + (ex + dx) % NX
-            send(
-                packed.at[rows_of(e)], gath.at[ty, line // LINES, rows_of(line % LINES * NX + ex)],
-                disp_send, disp_recv.at[line // LINES], e, tp,
-            )
+    def dispatch(buf, y, send_sem, recv_sem):
+        sends = tuple(enumerate(ORDER))
+        for line, dz in reversed(sends) if SEND_FAR else sends:
+            line = own_line if ABSOLUTE else line
+
+            @pl.loop(1 if dz == 0 else 0, NX)
+            def _(dx):
+                e = ((ez + NZ - dz) % NZ) * NX + (ex + dx) % NX
+                send(
+                    buf.at[rows_of(e)], gath.at[y, line // LINES, rows_of(line % LINES * NX + ex)],
+                    send_sem, recv_sem.at[line // LINES], e, tp,
+                )
+
+    dispatch(packed, ty, disp_send, disp_recv)
 
     for d in range(1, NT):
         t = (tp + d) % NT
@@ -135,12 +143,28 @@
 
     send(gate_h.at[1 - tc], wall.at[0, tc], wall_send, wall_recv, ep, mate)
     send(up_h.at[1 - tc], wall.at[1, tc], wall_send, wall_recv, ep, mate)
+
+    far = (ty + 2) % NY
+    if FAR_AT == 0:
+        pack(far, spare)
+        dispatch(spare, far, far_send, far_recv)
 
     with jax.named_scope("p_combine"):
         place, weights = placed(lax.broadcasted_iota(jnp.int32, (NE * NC, rows), 0))
         w_slots = jnp.where(place, weights[:, None, :], 0.0).reshape(NE * block, rows)
         combine[...] = w_slots.T
 
+    with jax.named_scope("p_columns"):
+        load_gate.wait()
+        load_up.wait()
+        arrived(wall.at[0], wall_recv)
+        for i in range(0, features, quarter):
+            columns[i : i + quarter, :] = wall[:, :, :, i : i + quarter].reshape(2 * NC * half, quarter).T
+
+    if FAR_AT == 1:
+        pack(far, spare)
+        dispatch(spare, far, far_send, far_recv)
+
     def share_out(buf, y, q, send_sem, recv_sem, to, part=None):
         ref = buf.at[y, q] if part is None else buf.at[y, q, part]
         send(ref, ref, send_sem, recv_sem, ep, to * NC + tc)
@@ -148,42 +172,30 @@
     def along(dy):
         return (ty + dy) % NY
 
-    halves = (pl.ds(0, chunk_rows // 2), pl.ds(chunk_rows // 2, chunk_rows // 2))
-
-    def stage_a(q):
+    def from_sources(y, q, recv_sem):
         @pl.when(own_q == q)
         def _():
-            arrived(gath.at[ty, q, pl.ds(0, chunk_rows - block)], disp_recv.at[q])
+            arrived(gath.at[y, q, pl.ds(0, chunk_rows - block)], recv_sem.at[q])
 
         @pl.when(own_q != q)
         def _():
-            arrived(gath.at[ty, q], disp_recv.at[q])
-
-        if not RELAY:
-            share_out(gath, ty, q, ag_send, ag_recv.at[ty, q], along(2))
+            arrived(gath.at[y, q], recv_sem.at[q])
+
+    def stage_a(q):
+        from_sources(ty, q, disp_recv)
         share_out(gath, ty, q, ag_send, ag_recv.at[ty, q], along(1))
         share_out(gath, ty, q, ag_send, ag_recv.at[ty, q], along(3))
 
-    def stage_b(q):
-        for here, there, part in ((3, 1, halves[0]), (1, 3, halves[1])):
-            arrived(gath.at[along(here), q], ag_recv.at[along(here), q])
-            if RELAY:
-                share_out(gath, along(here), q, ag_send, ag_recv.at[along(here), q], along(there), part)
-
     def stage_d(q):
-        if q == 0:
-            load_gate.wait()
-            load_up.wait()
-            arrived(wall.at[0], wall_recv)
-        arrived(gath.at[along(2), q], ag_recv.at[along(2), q])
+        from_sources(far, q, far_recv)
+        for dy in (1, 3):
+            arrived(gath.at[along(dy), q], ag_recv.at[along(dy), q])
         parts = []
         for y in range(NY):
             both = gath[y, q].astype(F32).reshape(PER, NC, cap, share)
             parts += [both[:, i].reshape(work_rows, share).astype(BF16) for i in range(NC)]
         x = jnp.concatenate(parts, axis=-1)
-        both = lax.dot_general(
-            x, wall[...].reshape(2 * NC * half, features), (((1,), (1,)), ((), ())), preferred_element_type=F32
-        )
+        both = jnp.dot(x, columns[...], preferred_element_type=F32)
         g, u = both[:, : NC * half], both[:, NC * half :]
         hid[ty, q] = (g / (1.0 + jnp.exp(-g)) * u).astype(BF16)
         for dy in (2, 1, 3):
@@ -229,7 +241,7 @@
                         t = ty * NC + c
                         send(outb.at[q, r, c], ret.at[ep * NC + tc], ret_send, ret_recv, e, t)
 
-    stages = {"a": stage_a, "b": stage_b, "d": stage_d, "f": stage_f}
+    stages = {"a": stage_a, "d": stage_d, "f": stage_f}
     for word in SEQ:
         with jax.named_scope(f"stage_{word}"):
             stages[word[0]](int(word[1:]))
@@ -252,7 +264,8 @@
         arrived(packed.at[pl.ds(0, (NE - 1) * block)], disp_send)
         arrived(wd.at[pl.ds(0, NT - 1)], wd_send)
         arrived(wall.at[0], wall_send)
-        arrived(gath.at[pl.ds(0, NY - 1)], ag_send)
+        arrived(gath.at[pl.ds(0, 2)], ag_send)
+        arrived(packed.at[pl.ds(0, (NE - 1) * block)], far_send)
         arrived(hid.at[pl.ds(0, NY - 1)], hid_send)
         arrived(ret.at[pl.ds(0, NE * NC - 1)], ret_send)
 
@@ -275,6 +288,8 @@
         scratch_shapes=[
             pltpu.VMEM((rows, features), BF16),
             pltpu.VMEM((2, NC, half, features), BF16),
+            pltpu.VMEM((features, 2 * NC * half), BF16),
+            pltpu.VMEM((NE * block, share), BF16),
             pltpu.VMEM((NE * block, share), BF16),
             pltpu.VMEM((NY, CHUNKS, PER * block, share), BF16),
             pltpu.VMEM((NT, half, quarter), BF16),
@@ -283,6 +298,8 @@
             pltpu.VMEM((NE * NC, cap + 1, 128), jnp.int32),
             pltpu.VMEM((rows, NE * block), F32),
             dma((4,)),
+            dma,
+            dma((CHUNKS,)),
             dma,
             dma((CHUNKS,)),
             dma,

time: 42.2 us -> 39.6 us (0.938)
  Pallas kernels: 41.1 us -> 38.8 us
    pallas_call x1, Pallas kernels: 41.1 us -> 38.8 us  [per_device(): pl.pallas_call(kernel, out_shape=pltpu.VMEM((rows, share), F32), in_specs...]
where the time goes in v5:
time: 39.6 us; the launch traced here: 39.4 us
  Pallas kernels  38.8 us (98%)
  other arithmetic  0.62 us (2%)
    pallas_call x1, Pallas kernels, per_device(): pl.pallas_call(kernel, out_shape=pltpu.VMEM((rows, share), F32), in_specs...  38.8 us

profile of v5, /device:TPU:1, one launch (start us, length us, event | category | flops | bytes accessed | tf_op | source)
XLA Modules:
  0.0 39.4 jit_solution(3131296576798532836)
XLA Ops:
  0.0 38.8 %shard_map.82 = f32[64,256]{1,0:T(8,128)S(1)} custom-call(bf16[64,2048]{1,0:T(8,128)(2,1)} %tokens_h.1, f32[1,2048]{1,0:T(1,128)} %bitcast.8, f32[1,2048]{1,0:T(1,128)} %bitcast.9, s32[4,64]{1,0:T(4,128)} %bitcast.10, f32[4,64]{1,0:T(4,128)} %bitcast.11, bf16[2,64,2048]{2,1,0:T(8,128)(2,1)} %bitcast.6, bf16[2,64,2048]{2,1,0:T(8,128)(2,1)} %bitcast.7, ...), custom_call_target="tpu_custom_call" | custom-call | tf_op jit(solution)/shard_map/pallas_call | solution.py:283
  38.8 0.6 %convert_element_type.3 = bf16[64,256]{1,0:T(8,128)(2,1)} convert(f32[64,256]{1,0:T(8,128)S(1)} %shard_map.82) | non-fusion elementwise | flops 16384 | bytes 98304 | tf_op jit(solution)/shard_map/convert_element_type | solution.py:327

commit v6 on v5

--- a/solution.py
+++ b/solution.py
@@ -17,7 +17,9 @@
 CHUNKS = 4
 LINES = NZ // CHUNKS
 PER = NE // CHUNKS
-FAR_AT = 0
+FAR_AT = 1
+WD_AT = 0
+FAR_FAR = True
 SEQ = ("a0", "a1", "a2", "a3", "d0", "d1", "d2", "d3", "f0", "f1", "f2", "f3")
 FINAL_CAST = True
 VMEM_LIMIT = 56 * 2**20
@@ -122,9 +124,9 @@
     with jax.named_scope("entry_wait"):
         pl.semaphore_wait(barrier, NE - 1 + NT - 1)
 
-    def dispatch(buf, y, send_sem, recv_sem):
+    def dispatch(buf, y, send_sem, recv_sem, farthest=SEND_FAR):
         sends = tuple(enumerate(ORDER))
-        for line, dz in reversed(sends) if SEND_FAR else sends:
+        for line, dz in reversed(sends) if farthest else sends:
             line = own_line if ABSOLUTE else line
 
             @pl.loop(1 if dz == 0 else 0, NX)
@@ -137,9 +139,13 @@
 
     dispatch(packed, ty, disp_send, disp_recv)
 
-    for d in range(1, NT):
-        t = (tp + d) % NT
-        send(down_h.at[t % NC, :, quarter_of(t // NC)], wd.at[tp], wd_send, wd_recv, ep, t)
+    def exchange_down():
+        for d in range(1, NT):
+            t = (tp + d) % NT
+            send(down_h.at[t % NC, :, quarter_of(t // NC)], wd.at[tp], wd_send, wd_recv, ep, t)
+
+    if WD_AT == 0:
+        exchange_down()
 
     send(gate_h.at[1 - tc], wall.at[0, tc], wall_send, wall_recv, ep, mate)
     send(up_h.at[1 - tc], wall.at[1, tc], wall_send, wall_recv, ep, mate)
@@ -147,12 +153,18 @@
     far = (ty + 2) % NY
     if FAR_AT == 0:
         pack(far, spare)
-        dispatch(spare, far, far_send, far_recv)
+        dispatch(spare, far, far_send, far_recv, FAR_FAR)
 
     with jax.named_scope("p_combine"):
-        place, weights = placed(lax.broadcasted_iota(jnp.int32, (NE * NC, rows), 0))
-        w_slots = jnp.where(place, weights[:, None, :], 0.0).reshape(NE * block, rows)
+        every, weights = placed(lax.broadcasted_iota(jnp.int32, (NE * NC, rows), 0))
+        w_slots = jnp.where(every, weights[:, None, :], 0.0).reshape(NE * block, rows)
         combine[...] = w_slots.T
+
+    if WD_AT == 1:
+        exchange_down()
+    if FAR_AT == 2:
+        pack(far, spare)
+        dispatch(spare, far, far_send, far_recv, FAR_FAR)
 
     with jax.named_scope("p_columns"):
         load_gate.wait()
@@ -163,7 +175,7 @@
 
     if FAR_AT == 1:
         pack(far, spare)
-        dispatch(spare, far, far_send, far_recv)
+        dispatch(spare, far, far_send, far_recv, FAR_FAR)
 
     def share_out(buf, y, q, send_sem, recv_sem, to, part=None):
         ref = buf.at[y, q] if part is None else buf.at[y, q, part]

time: 39.6 us -> 39 us (0.985)
  Pallas kernels: 38.8 us -> 37.9 us
    pallas_call x1, Pallas kernels: 38.8 us -> 37.9 us  [per_device(): pl.pallas_call(kernel, out_shape=pltpu.VMEM((rows, share), F32), in_specs...]
where the time goes in v6:
time: 39 us; the launch traced here: 38.6 us
  Pallas kernels  37.9 us (97%)
  other arithmetic  0.62 us (2%)
    pallas_call x1, Pallas kernels, per_device(): pl.pallas_call(kernel, out_shape=pltpu.VMEM((rows, share), F32), in_specs...  37.9 us

profile of v6, /device:TPU:1, one launch (start us, length us, event | category | flops | bytes accessed | tf_op | source)
XLA Modules:
  0.0 38.6 jit_solution(6860415322989213250)
XLA Ops:
  0.0 37.9 %shard_map.82 = f32[64,256]{1,0:T(8,128)S(1)} custom-call(bf16[64,2048]{1,0:T(8,128)(2,1)} %tokens_h.1, f32[1,2048]{1,0:T(1,128)} %bitcast.8, f32[1,2048]{1,0:T(1,128)} %bitcast.9, s32[4,64]{1,0:T(4,128)} %bitcast.10, f32[4,64]{1,0:T(4,128)} %bitcast.11, bf16[2,64,2048]{2,1,0:T(8,128)(2,1)} %bitcast.6, bf16[2,64,2048]{2,1,0:T(8,128)(2,1)} %bitcast.7, ...), custom_call_target="tpu_custom_call" | custom-call | tf_op jit(solution)/shard_map/pallas_call | solution.py:295
  37.9 0.6 %convert_element_type.3 = bf16[64,256]{1,0:T(8,128)(2,1)} convert(f32[64,256]{1,0:T(8,128)S(1)} %shard_map.82) | non-fusion elementwise | flops 16384 | bytes 98304 | tf_op jit(solution)/shard_map/convert_element_type | solution.py:339

commit v7 on v6

--- a/solution.py
+++ b/solution.py
@@ -10,7 +10,7 @@
 NZ, NX, NY, NC = 8, 4, 4, 2
 NE, NT = NZ * NX, NY * NC
 ABSOLUTE = True
-ZORDER = (0, 1, 2, 3, 4, 5, 6, 7)
+ZORDER = (0, 4, 1, 5, 2, 6, 3, 7)
 SEND_FAR = True
 SIG_FAR = True
 ORDER = (0, 7, 1, 6, 2, 5, 3, 4)
@@ -27,6 +27,21 @@
 LEVELS = 32760.0
 KEYS = 128.0
 F32, BF16 = jnp.float32, jnp.bfloat16
+
+
+def weighted(weights, codes):
+    high = (codes + 128) >> 8
+    low = codes - (high << 8)
+    parts, rest = [], weights
+    for _ in range(3):
+        parts.append(rest.astype(BF16))
+        rest = rest - parts[-1].astype(F32)
+    left = jnp.concatenate(parts, axis=0)
+    right = jnp.concatenate([high.astype(F32).astype(BF16), low.astype(F32).astype(BF16)], axis=-1)
+    terms = jnp.dot(left, right, preferred_element_type=F32)
+    n, m = weights.shape[0], codes.shape[1]
+    terms = terms[:n] + terms[n : 2 * n] + terms[2 * n :]
+    return terms[:, :m] * 256.0 + terms[:, m:]
 
 
 def kernel(
@@ -75,7 +90,7 @@
     def signal(e, t):
         pl.semaphore_signal(barrier, inc=1, device_id=(e, t), device_id_type=MESH)
 
-    for dz in (4, 3, 5, 2, 6, 1, 7, 0):
+    for dz in (0, 1, 7, 2, 6, 3, 5, 4):
         for dx in range(1 if dz == 0 else 0, NX):
             signal(((ez + dz) % NZ) * NX + (ex + dx) % NX, tp)
     for d in range(1, NT):
@@ -156,9 +171,11 @@
         dispatch(spare, far, far_send, far_recv, FAR_FAR)
 
     with jax.named_scope("p_combine"):
-        every, weights = placed(lax.broadcasted_iota(jnp.int32, (NE * NC, rows), 0))
+        number = lax.broadcasted_iota(jnp.int32, (NE * NC, rows), 0)
+        every, weights = placed(number % NE * NC + number // NE)
         w_slots = jnp.where(every, weights[:, None, :], 0.0).reshape(NE * block, rows)
-        combine[...] = w_slots.T
+        for c in range(NC):
+            combine[c] = w_slots[c * NE * cap : (c + 1) * NE * cap].T
 
     if WD_AT == 1:
         exchange_down()
@@ -226,18 +243,18 @@
         for c in range(NC):
             left = level[:, c * share : c * share + 128]
             right = level[:, c * share + 128 : (c + 1) * share]
-            outb[q, :, c, 0:cap, :] = ((left << 16) | (right & 0xFFFF)).reshape(PER, cap, 128)
+            outb[pl.ds(c * NE + q * PER, PER), 0:cap, :] = ((left << 16) | (right & 0xFFFF)).reshape(PER, cap, 128)
         row = lax.broadcasted_iota(jnp.int32, (work_rows, 128), 0) % cap
         col = lax.broadcasted_iota(jnp.int32, (work_rows, 128), 1)
-        keys = jnp.where(col == row + tc * cap + ep % (128 // block) * block, key, 0.0)
+        keys = jnp.where(col == row + ep % (128 // cap) * cap, key, 0.0)
         keys = jnp.sum(keys.reshape(PER, cap, 128), axis=1, keepdims=True).astype(jnp.int32)
         for c in range(NC):
-            outb[q, :, c, cap : cap + 1, :] = keys
+            outb[pl.ds(c * NE + q * PER, PER), cap : cap + 1, :] = keys
 
         @pl.when(own_q == q)
         def _():
             r = own_line % LINES * NX + ex
-            ret[ep * NC + tc] = outb[q, r, tc]
+            ret[tc, ep] = outb[tc * NE + q * PER + r]
 
         for k in range(LINES):
             line = q * LINES + k
@@ -251,26 +268,33 @@
                     @pl.when((e != ep) | (c != tc))
                     def _():
                         t = ty * NC + c
-                        send(outb.at[q, r, c], ret.at[ep * NC + tc], ret_send, ret_recv, e, t)
+                        send(outb.at[c * NE + q * PER + r], ret.at[tc, ep], ret_send, ret_recv.at[tc], e, t)
 
     stages = {"a": stage_a, "d": stage_d, "f": stage_f}
     for word in SEQ:
         with jax.named_scope(f"stage_{word}"):
             stages[word[0]](int(word[1:]))
 
-    with jax.named_scope("ret_wait"):
-        arrived(ret.at[pl.ds(0, NE * NC - 1)], ret_recv)
-    per = 128 // block
-    words = ret[:, 0:cap, :].reshape(NE * block, 128)
-    back = jnp.concatenate([words >> 16, (words << 16) >> 16], axis=-1).astype(F32)
-    keys = ret[:, cap : cap + 1, :].astype(F32)
-    keys = jnp.concatenate(
-        [jnp.sum(keys[i * per * NC : (i + 1) * per * NC], axis=0) for i in range(NE // per)], axis=-1
-    )
-    scale = jnp.exp2(keys * (1.0 / KEYS)) * (1.0 / LEVELS)
-    out_v[...] = jnp.dot(
-        combine[...] * scale, back, preferred_element_type=F32, precision=lax.Precision.HIGHEST
-    ).astype(out_v.dtype)
+    per = 128 // cap
+    total = jnp.zeros(out_v.shape, F32)
+    for c in (1, 0):
+        with jax.named_scope(f"ret_wait{c}"):
+
+            @pl.when(tc == c)
+            def _():
+                arrived(ret.at[c, pl.ds(0, NE - 1)], ret_recv.at[c])
+
+            @pl.when(tc != c)
+            def _():
+                arrived(ret.at[c], ret_recv.at[c])
+
+        words = ret[c, :, 0:cap, :].reshape(NE * cap, 128)
+        back = jnp.concatenate([words >> 16, (words << 16) >> 16], axis=-1)
+        keys = ret[c, :, cap : cap + 1, :].astype(F32)
+        keys = jnp.concatenate([jnp.sum(keys[i : i + per], axis=0) for i in range(0, NE, per)], axis=-1)
+        scale = jnp.exp2(keys * (1.0 / KEYS)) * (1.0 / LEVELS)
+        total = total + weighted(combine[c] * scale, back)
+    out_v[...] = total.astype(out_v.dtype)
 
     with jax.named_scope("drain"):
         arrived(packed.at[pl.ds(0, (NE - 1) * block)], disp_send)
@@ -279,7 +303,7 @@
         arrived(gath.at[pl.ds(0, 2)], ag_send)
         arrived(packed.at[pl.ds(0, (NE - 1) * block)], far_send)
         arrived(hid.at[pl.ds(0, NY - 1)], hid_send)
-        arrived(ret.at[pl.ds(0, NE * NC - 1)], ret_send)
+        arrived(outb.at[pl.ds(0, NE * NC - 1)], ret_send)
 
 
 def per_device(tokens, norm_gain, norm_shift, expert_ids, gate_weights, expert_gate, expert_up, expert_down):
@@ -306,9 +330,9 @@
             pltpu.VMEM((NY, CHUNKS, PER * block, share), BF16),
             pltpu.VMEM((NT, half, quarter), BF16),
             pltpu.VMEM((NY, CHUNKS, PER * cap, NC * half), BF16),
-            pltpu.VMEM((CHUNKS, PER, NC, cap + 1, 128), jnp.int32),
             pltpu.VMEM((NE * NC, cap + 1, 128), jnp.int32),
-            pltpu.VMEM((rows, NE * block), F32),
+            pltpu.VMEM((NC, NE, cap + 1, 128), jnp.int32),
+            pltpu.VMEM((NC, rows, NE * cap), F32),
             dma((4,)),
             dma,
             dma((CHUNKS,)),
@@ -323,7 +347,7 @@
             dma,
             dma((CHUNKS,)),
             dma,
-            dma,
+            dma((NC,)),
         ],
         compiler_params=pltpu.CompilerParams(collective_id=0, has_side_effects=True, vmem_limit_bytes=VMEM_LIMIT),
     )(

time: 39 us -> 39.1 us (level)
  the two profiles are of different devices: /device:TPU:1 before, /device:TPU:97 now
where the time goes in v7:
time: 39.1 us; the launch traced here: 38.9 us
  Pallas kernels  38.3 us (98%)
  other arithmetic  0.62 us (2%)
    pallas_call x1, Pallas kernels, per_device(): pl.pallas_call(kernel, out_shape=pltpu.VMEM((rows, share), F32), in_specs...  38.3 us

profile of v7, /device:TPU:97, one launch (start us, length us, event | category | flops | bytes accessed | tf_op | source)
XLA Modules:
  0.0 38.9 jit_solution(1635038811419148524)
XLA Ops:
  0.0 38.3 %shard_map.82 = f32[64,256]{1,0:T(8,128)S(1)} custom-call(bf16[64,2048]{1,0:T(8,128)(2,1)} %tokens_h.1, f32[1,2048]{1,0:T(1,128)} %bitcast.8, f32[1,2048]{1,0:T(1,128)} %bitcast.9, s32[4,64]{1,0:T(4,128)} %bitcast.10, f32[4,64]{1,0:T(4,128)} %bitcast.11, bf16[2,64,2048]{2,1,0:T(8,128)(2,1)} %bitcast.6, bf16[2,64,2048]{2,1,0:T(8,128)(2,1)} %bitcast.7, ...), custom_call_target="tpu_custom_call" | custom-call | tf_op jit(solution)/shard_map/pallas_call | solution.py:319
  38.3 0.6 %convert_element_type.3 = bf16[64,256]{1,0:T(8,128)(2,1)} convert(f32[64,256]{1,0:T(8,128)S(1)} %shard_map.82) | non-fusion elementwise | flops 16384 | bytes 98304 | tf_op jit(solution)/shard_map/convert_element_type | solution.py:363

commit v8 on v7

--- a/solution.py
+++ b/solution.py
@@ -93,7 +93,7 @@
     for dz in (0, 1, 7, 2, 6, 3, 5, 4):
         for dx in range(1 if dz == 0 else 0, NX):
             signal(((ez + dz) % NZ) * NX + (ex + dx) % NX, tp)
-    for d in range(1, NT):
+    for d in (2, 4, 6, 1, 3, 5, 7):
         signal(ep, (tp + d) % NT)
 
     ids, gw = ids_v[...], gw_v[...]
@@ -155,7 +155,7 @@
     dispatch(packed, ty, disp_send, disp_recv)
 
     def exchange_down():
-        for d in range(1, NT):
+        for d in (2, 4, 6, 1, 3, 5, 7):
             t = (tp + d) % NT
             send(down_h.at[t % NC, :, quarter_of(t // NC)], wd.at[tp], wd_send, wd_recv, ep, t)
 

time: 39.1 us -> 39 us (level)
  the two profiles are of different devices: /device:TPU:97 before, /device:TPU:1 now
where the time goes in v8:
time: 39 us; the launch traced here: 38.9 us
  Pallas kernels  38.3 us (98%)
  other arithmetic  0.62 us (2%)
    pallas_call x1, Pallas kernels, per_device(): pl.pallas_call(kernel, out_shape=pltpu.VMEM((rows, share), F32), in_specs...  38.3 us

profile of v8, /device:TPU:1, one launch (start us, length us, event | category | flops | bytes accessed | tf_op | source)
XLA Modules:
  0.0 38.9 jit_solution(2999123933680495690)
XLA Ops:
  0.0 38.3 %shard_map.82 = f32[64,256]{1,0:T(8,128)S(1)} custom-call(bf16[64,2048]{1,0:T(8,128)(2,1)} %tokens_h.1, f32[1,2048]{1,0:T(1,128)} %bitcast.8, f32[1,2048]{1,0:T(1,128)} %bitcast.9, s32[4,64]{1,0:T(4,128)} %bitcast.10, f32[4,64]{1,0:T(4,128)} %bitcast.11, bf16[2,64,2048]{2,1,0:T(8,128)(2,1)} %bitcast.6, bf16[2,64,2048]{2,1,0:T(8,128)(2,1)} %bitcast.7, ...), custom_call_target="tpu_custom_call" | custom-call | tf_op jit(solution)/shard_map/pallas_call | solution.py:319
  38.3 0.6 %convert_element_type.3 = bf16[64,256]{1,0:T(8,128)(2,1)} convert(f32[64,256]{1,0:T(8,128)S(1)} %shard_map.82) | non-fusion elementwise | flops 16384 | bytes 98304 | tf_op jit(solution)/shard_map/convert_element_type | solution.py:363

commit v9 on v8

--- a/solution.py
+++ b/solution.py
@@ -212,8 +212,8 @@
 
     def stage_a(q):
         from_sources(ty, q, disp_recv)
+        share_out(gath, ty, q, ag_send, ag_recv.at[ty, q], along(3))
         share_out(gath, ty, q, ag_send, ag_recv.at[ty, q], along(1))
-        share_out(gath, ty, q, ag_send, ag_recv.at[ty, q], along(3))
 
     def stage_d(q):
         from_sources(far, q, far_recv)

time: 39 us -> 39.1 us (level)
  no operation moved by 1% of the time
where the time goes in v9:
time: 39.1 us; the launch traced here: 38.9 us
  Pallas kernels  38.3 us (98%)
  other arithmetic  0.62 us (2%)
    pallas_call x1, Pallas kernels, per_device(): pl.pallas_call(kernel, out_shape=pltpu.VMEM((rows, share), F32), in_specs...  38.3 us

profile of v9, /device:TPU:1, one launch (start us, length us, event | category | flops | bytes accessed | tf_op | source)
XLA Modules:
  0.0 38.9 jit_solution(15621060609192249649)
XLA Ops:
  0.0 38.3 %shard_map.82 = f32[64,256]{1,0:T(8,128)S(1)} custom-call(bf16[64,2048]{1,0:T(8,128)(2,1)} %tokens_h.1, f32[1,2048]{1,0:T(1,128)} %bitcast.8, f32[1,2048]{1,0:T(1,128)} %bitcast.9, s32[4,64]{1,0:T(4,128)} %bitcast.10, f32[4,64]{1,0:T(4,128)} %bitcast.11, bf16[2,64,2048]{2,1,0:T(8,128)(2,1)} %bitcast.6, bf16[2,64,2048]{2,1,0:T(8,128)(2,1)} %bitcast.7, ...), custom_call_target="tpu_custom_call" | custom-call | tf_op jit(solution)/shard_map/pallas_call | solution.py:319
  38.3 0.6 %convert_element_type.3 = bf16[64,256]{1,0:T(8,128)(2,1)} convert(f32[64,256]{1,0:T(8,128)S(1)} %shard_map.82) | non-fusion elementwise | flops 16384 | bytes 98304 | tf_op jit(solution)/shard_map/convert_element_type | solution.py:363

commit v10 on v8

--- a/solution.py
+++ b/solution.py
@@ -159,11 +159,12 @@
             t = (tp + d) % NT
             send(down_h.at[t % NC, :, quarter_of(t // NC)], wd.at[tp], wd_send, wd_recv, ep, t)
 
+    send(gate_h.at[1 - tc], wall.at[0, tc], wall_send, wall_recv, ep, mate)
+    send(up_h.at[1 - tc], wall.at[1, tc], wall_send, wall_recv, ep, mate)
+
     if WD_AT == 0:
         exchange_down()
 
-    send(gate_h.at[1 - tc], wall.at[0, tc], wall_send, wall_recv, ep, mate)
-    send(up_h.at[1 - tc], wall.at[1, tc], wall_send, wall_recv, ep, mate)
 
     far = (ty + 2) % NY
     if FAR_AT == 0:

time: 39 us -> 39 us (level)
  no operation moved by 1% of the time
where the time goes in v10:
time: 39 us; the launch traced here: 38.8 us
  Pallas kernels  38.2 us (98%)
  other arithmetic  0.62 us (2%)
    pallas_call x1, Pallas kernels, per_device(): pl.pallas_call(kernel, out_shape=pltpu.VMEM((rows, share), F32), in_specs...  38.2 us

profile of v10, /device:TPU:1, one launch (start us, length us, event | category | flops | bytes accessed | tf_op | source)
XLA Modules:
  0.0 38.8 jit_solution(14984987583332998053)
XLA Ops:
  0.0 38.2 %shard_map.82 = f32[64,256]{1,0:T(8,128)S(1)} custom-call(bf16[64,2048]{1,0:T(8,128)(2,1)} %tokens_h.1, f32[1,2048]{1,0:T(1,128)} %bitcast.8, f32[1,2048]{1,0:T(1,128)} %bitcast.9, s32[4,64]{1,0:T(4,128)} %bitcast.10, f32[4,64]{1,0:T(4,128)} %bitcast.11, bf16[2,64,2048]{2,1,0:T(8,128)(2,1)} %bitcast.6, bf16[2,64,2048]{2,1,0:T(8,128)(2,1)} %bitcast.7, ...), custom_call_target="tpu_custom_call" | custom-call | tf_op jit(solution)/shard_map/pallas_call | solution.py:320
  38.2 0.6 %convert_element_type.3 = bf16[64,256]{1,0:T(8,128)(2,1)} convert(f32[64,256]{1,0:T(8,128)S(1)} %shard_map.82) | non-fusion elementwise | flops 16384 | bytes 98304 | tf_op jit(solution)/shard_map/convert_element_type | solution.py:364
